TPU v7x, 512 devices: a whole 4x8x8 slice. The times are simulated.
512 devices in a mesh: ep: 128 (over z, y, core), tp: 4 (over x).
Axes of the slice: x: 4, y: 8, z: 8, core: 2. Of those that a mesh axis runs over, the one named last changes fastest.
Arguments:
- tokens: bfloat16 [2048, 2048], P('ep'), may hold values from -6 to 6
- positions: int32 [2048], P('ep'), may hold values from 1024 to 16383
- state: float32 [2048, 4, 128, 128], P('ep', 'tp'), may hold values from -1 to 1
- mix_gain: float32 [2048], replicated, may hold values from 0.1 to 1.9
- w_query: bfloat16 [2048, 512], P(None, 'tp'), may hold values from -0.125 to 0.125
- w_key: bfloat16 [2048, 512], P(None, 'tp'), may hold values from -0.125 to 0.125
- w_value: bfloat16 [2048, 512], P(None, 'tp'), may hold values from -0.125 to 0.125
- w_out: bfloat16 [512, 2048], P('tp'), may hold values from -0.25 to 0.25
- ffn_gain: float32 [2048], replicated, may hold values from 0.1 to 1.9
- branch_gate: bfloat16 [2048], replicated, may hold values from -0.125 to 0.125
- dense_gate: bfloat16 [2048, 4096], P('tp', 'ep'), may hold values from -0.125 to 0.125
- dense_up: bfloat16 [2048, 4096], P('tp', 'ep'), may hold values from -0.125 to 0.125
- dense_down: bfloat16 [4096, 2048], P('ep', 'tp'), may hold values from -0.09375 to 0.09375
- routes: int32 [2048, 6], P('ep'), may hold values from 0 to 127, all different within a row; in each aligned block of 16 rows (0 to 15, 16 to 31, ...) at most 2 rows name the same one
- route_scores: float32 [2048, 6], P('ep'), may hold values from 0.05 to 1
- expert_gate: bfloat16 [128, 2048, 512], P('ep', None, 'tp'), may hold values from -0.125 to 0.125
- expert_up: bfloat16 [128, 2048, 512], P('ep', None, 'tp'), may hold values from -0.125 to 0.125
- expert_down: bfloat16 [128, 512, 2048], P('ep', 'tp'), may hold values from -0.25 to 0.25
Outputs:
- layer_out: bfloat16 [2048, 2048], P('ep', 'tp')
Inputs may be any that keep to these rules, and one draw needn't show every extreme that they name: `routes`: each row names 6 different experts. In each aligned block of 16 rows (the rows of one index of ep) no expert is named by more than 2 rows, a bound that some block reaches.
All inputs are finite; a program needn't handle non-finite values.
Results may differ from a plain program's by a relative error of at most 0.012.
Values may be sent and summed in bfloat16 or wider, within the bound.
A program may use at most 64 MiB of HBM per device.

v0:
```python
import jax
import jax.numpy as jnp
from jax import lax
from jax.sharding import PartitionSpec as P

EPS = 1e-06


def from_everyone(shard, axis):
    copies = jnp.broadcast_to(shard, (lax.axis_size(axis), *shard.shape))
    return lax.all_to_all(copies, axis, split_axis=0, concat_axis=0, tiled=True)


def of_everyone(shard, axis):
    return from_everyone(shard, axis).astype(jnp.float32).sum(axis=0)


def normalize(inputs, scale_vec):
    values = inputs.astype(jnp.float32)
    return values * lax.rsqrt(jnp.mean(values * values, axis=-1, keepdims=True) + EPS) * scale_vec


def rotate(vectors, where):
    half = vectors.shape[-1] // 2
    inverse = 1.0 / 10000.0 ** jnp.linspace(0.0, 1.0, half, dtype=jnp.float32)
    angle = where.astype(jnp.float32)[:, None] * inverse[None, :]
    cosine = jnp.cos(angle)[:, None, :]
    sine = jnp.sin(angle)[:, None, :]
    first = vectors[..., :half]
    second = vectors[..., half:]
    return jnp.concatenate(
        [first * cosine - second * sine, second * cosine + first * sine], axis=-1
    )


def on_device(
    tokens,
    positions,
    state,
    mix_gain,
    w_query,
    w_key,
    w_value,
    w_out,
    ffn_gain,
    branch_gate,
    dense_gate,
    dense_up,
    dense_down,
    routes,
    route_scores,
    expert_gate,
    expert_up,
    expert_down,
):
    sequences = tokens.shape[0]
    model_width = tokens.shape[1]
    tp_count = lax.axis_size("tp")
    ep_count = lax.axis_size("ep")
    columns = model_width // tp_count
    tp_index = lax.axis_index("tp")
    local_heads = state.shape[1]
    head_dim = state.shape[2]
    normed = normalize(tokens, mix_gain).astype(jnp.bfloat16)
    query_vec = jnp.dot(normed, w_query, preferred_element_type=jnp.float32).reshape(
        sequences, local_heads, head_dim
    )
    key_vec = jnp.dot(normed, w_key, preferred_element_type=jnp.float32).reshape(
        sequences, local_heads, head_dim
    )
    value_vec = jnp.dot(normed, w_value, preferred_element_type=jnp.float32).reshape(
        sequences, local_heads, head_dim
    )
    query_vec = rotate(query_vec, positions)
    key_vec = rotate(key_vec, positions) * head_dim ** (-0.5)
    all_heads = local_heads * tp_count
    head_index = (tp_index * local_heads + jnp.arange(local_heads, dtype=jnp.int32)).astype(
        jnp.float32
    )
    decay_rate = 1.0 - 2.0 ** (-5.0 - 5.0 * head_index / (all_heads - 1))
    new_state = (
        decay_rate[None, :, None, None] * state + key_vec[:, :, :, None] * value_vec[:, :, None, :]
    )
    retrieved = jnp.einsum("bhd,bhde->bhe", query_vec, new_state)
    retrieved = retrieved * lax.rsqrt(jnp.mean(retrieved * retrieved, axis=-1, keepdims=True) + EPS)
    retrieved = retrieved.reshape(sequences, local_heads * head_dim).astype(jnp.bfloat16)
    head_partial = jnp.dot(retrieved, w_out, preferred_element_type=jnp.float32).astype(
        jnp.bfloat16
    )
    mixer_out = of_everyone(head_partial.astype(jnp.float32).astype(jnp.bfloat16), "tp").astype(
        jnp.float32
    )
    after_mix = tokens.astype(jnp.float32) + mixer_out
    ffn_in = normalize(after_mix, ffn_gain).astype(jnp.bfloat16)
    own_cols = lax.dynamic_slice_in_dim(ffn_in, tp_index * columns, columns, 1)
    per_device = expert_gate.shape[0]
    experts = per_device * ep_count
    fanout = routes.shape[1]
    capacity = max(2, min(sequences, 2 * sequences * fanout // experts))
    slot_count = experts * capacity
    marks = (routes[:, :, None] == jnp.arange(experts, dtype=jnp.int32)[None, None, :]).astype(
        jnp.int32
    )
    flattened = marks.reshape(sequences * fanout, experts)
    ranking = jnp.sum((jnp.cumsum(flattened, axis=0) - flattened) * flattened, axis=1).reshape(
        sequences, fanout
    )
    slot_index = routes * capacity + ranking
    matches = jnp.arange(slot_count, dtype=jnp.int32)[:, None, None] == slot_index[None]
    placing = jnp.any(matches, axis=2).astype(jnp.bfloat16)
    route_weights = route_scores / jnp.sum(route_scores, axis=1, keepdims=True)
    combining = jnp.sum(jnp.where(matches, route_weights[None], 0.0), axis=2).T
    packed = jnp.dot(placing, ffn_in, preferred_element_type=jnp.float32).astype(jnp.bfloat16)
    packed = packed.reshape(experts, capacity, ffn_in.shape[1])
    received = lax.all_to_all(packed, "ep", split_axis=0, concat_axis=0, tiled=True)
    count = received.shape[1]
    grouped = received.reshape(ep_count, per_device, count, model_width)
    gate_pre = jnp.einsum(
        "skcd,kdw->skcw", grouped, expert_gate, preferred_element_type=jnp.float32
    )
    up_pre = jnp.einsum("skcd,kdw->skcw", grouped, expert_up, preferred_element_type=jnp.float32)
    hidden = (jax.nn.silu(gate_pre) * up_pre).astype(jnp.bfloat16)
    partial_out = jnp.einsum(
        "skcw,kwd->skcd", hidden, expert_down, preferred_element_type=jnp.float32
    )
    blocks_out = partial_out.astype(jnp.bfloat16).reshape(
        ep_count, per_device, count, tp_count, columns
    )
    traded = lax.all_to_all(blocks_out, "tp", split_axis=3, concat_axis=3, tiled=True)
    mine = jnp.sum(traded.astype(jnp.float32), axis=3).astype(jnp.bfloat16)
    mine = mine.reshape(ep_count * per_device, count, columns)
    returned = lax.all_to_all(mine, "ep", split_axis=0, concat_axis=0, tiled=True)
    experts_out = jnp.dot(combining, returned.reshape(slot_count, columns).astype(jnp.float32))
    hidden_units = dense_gate.shape[1]
    both_weights = jnp.concatenate([dense_gate, dense_up], axis=1)
    pre_parts = jnp.dot(
        lax.all_gather(own_cols, "ep", axis=0, tiled=True),
        both_weights,
        preferred_element_type=jnp.float32,
    ).astype(jnp.bfloat16)
    pre_total = of_everyone(pre_parts.astype(jnp.float32).astype(jnp.bfloat16), "tp").astype(
        jnp.float32
    )
    dense_hidden = (jax.nn.silu(pre_total[:, :hidden_units]) * pre_total[:, hidden_units:]).astype(
        jnp.bfloat16
    )
    own_hidden = lax.all_to_all(dense_hidden, "ep", split_axis=0, concat_axis=1, tiled=True)
    dense_out = jnp.dot(
        own_hidden,
        lax.all_gather(dense_down, "ep", axis=0, tiled=True),
        preferred_element_type=jnp.float32,
    )
    branch_weight = jax.nn.sigmoid(jnp.dot(ffn_in, branch_gate, preferred_element_type=jnp.float32))
    residual_cols = lax.dynamic_slice_in_dim(after_mix, tp_index * columns, columns, 1)
    layer_out = residual_cols + experts_out + branch_weight[:, None] * dense_out
    return layer_out.astype(jnp.bfloat16)


def solution(mesh):
    placed = (
        P("ep", None),
        P("ep"),
        P("ep", "tp", None, None),
        P(),
        P(None, "tp"),
        P(None, "tp"),
        P(None, "tp"),
        P("tp", None),
        P(),
        P(),
        P("tp", "ep"),
        P("tp", "ep"),
        P("ep", "tp"),
        P("ep", None),
        P("ep", None),
        P("ep", None, "tp"),
        P("ep", None, "tp"),
        P("ep", "tp", None),
    )
    return jax.shard_map(
        on_device, mesh=mesh, in_specs=placed, out_specs=P("ep", "tp"), check_vma=False
    )
```

profile of v0, /device:TPU:1, one launch (start us, length us, event | category | flops | bytes accessed | tf_op | source)
XLA Modules:
  0.0 224.6 jit_solution(2779366031340927254)
XLA Ops:
  6.6 1.1 fusion.26
  7.7 0.7 convert_element_type.71
  8.3 1.3 convolution_bitcast_fusion.2
  9.7 1.4 convolution_bitcast_fusion.3
  11.1 1.3 fusion.58
  12.5 0.1 fusion.51
  12.8 0.4 fusion.9
  13.3 0.1 multiply_reduce_fusion.1
  13.4 0.2 convolution_convert_fusion.3
  13.7 0.7 broadcast_in_dim.13
  14.4 4.8 %all-to-all-start = ((bf16[4,16,2048]{2,1,0:T(8,128)(2,1)}), bf16[4,16,2048]{2,1,0:T(8,128)(2,1)S(1)}, u32[]{:S(2)}, u32[]{:S(2)}) async-start(bf16[4,16,2048]{2,1,0:T(8,128)(2,1)} %broadcast_in_dim.13), calls=%async_computation | async-start | bytes 524288 | tf_op jit(solution)/shard_map/all_to_all | solution.py:11
  19.2 5.5 %all-to-all-done = bf16[4,16,2048]{2,1,0:T(8,128)(2,1)S(1)} async-done(((bf16[4,16,2048]{2,1,0:T(8,128)(2,1)}), bf16[4,16,2048]{2,1,0:T(8,128)(2,1)S(1)}, u32[]{:S(2)}, u32[]{:S(2)}) %all-to-all-start) | async-done | bytes 262176 | tf_op jit(solution)/shard_map/all_to_all | solution.py:11
  24.8 0.1 multiply_reduce_fusion
  25.0 0.6 constant_dynamic-slice_fusion
  25.7 0.7 all-gather.5.cloned.1.call-update
  26.7 0.1 reduce_window_sum.11
  26.9 0.2 select_reduce_fusion.1
  27.1 0.1 copy.73
  27.2 0.1 fusion.34
  27.3 0.5 convolution_convert_fusion.1
  27.8 0.7 reshape.226
  28.5 50.3 %all_to_all.44 = bf16[128,2,2048]{2,1,0:T(2,128)(2,1)S(1)} all-to-all(bf16[128,2,2048]{2,1,0:T(2,128)(2,1)S(1)} %reshape.226), channel_id=1, replica_groups=mesh['ep'=128,'tp'=4] {'ep'}, dimensions={0} | all-to-all | bytes 2097152 | tf_op jit(solution)/shard_map/all_to_all | solution.py:115
  78.9 1.8 convolution_bitcast_fusion.1
  80.7 1.1 convolution_convert_fusion
  81.8 1.1 copy.92
  82.9 3.5 %all-to-all-start.2 = ((bf16[128,1,2,4,512]{4,0,2,1,3:T(8,128)(2,1)}), bf16[128,1,2,4,512]{4,0,2,1,3:T(8,128)(2,1)S(1)}, u32[]{:S(2)}, u32[]{:S(2)}) async-start(bf16[128,1,2,4,512]{4,0,2,1,3:T(8,128)(2,1)} %bitcast.91), calls=%async_computation.2 | async-start | bytes 2097152 | tf_op jit(solution)/shard_map/all_to_all | solution.py:129
  86.4 40.0 %all-gather.3.cloned.1.call-done = bf16[2048,512]{1,0:T(8,128)(2,1)} async-done(((bf16[16,512]{1,0:T(8,128)(2,1)}), bf16[2048,512]{1,0:T(8,128)(2,1)}) %all-gather.3.cloned.1.call-update) | async-done | bytes 2097168 | tf_op jit(solution)/shard_map/all_gather | solution.py:137
  126.4 2.3 %convolution_convert_fusion.2 = bf16[2048,64]{0,1:T(8,128)(2,1)S(1)} fusion(bf16[2048,512]{1,0:T(8,128)(2,1)} %all-gather.3.cloned.1.call-done, bf16[512,32]{0,1:T(8,128)(2,1)S(1)} %copy-done.7, bf16[512,32]{0,1:T(8,128)(2,1)S(1)} %copy-done.8), kind=kOutput, calls=%fused_computation.2 | convolution fusion | flops 134479872 | bytes 2424832 | tf_op jit(solution)/shard_map/dot_general | solution.py:136
  128.8 1.1 broadcast_in_dim.16
  129.9 4.0 %all-to-all-start.4 = ((bf16[4,2048,64]{1,2,0:T(8,128)(2,1)}), bf16[4,2048,64]{1,2,0:T(8,128)(2,1)S(1)}, u32[]{:S(2)}, u32[]{:S(2)}) async-start(bf16[4,2048,64]{1,2,0:T(8,128)(2,1)} %broadcast_in_dim.16), calls=%async_computation.4 | async-start | bytes 2097152 | tf_op jit(solution)/shard_map/all_to_all | solution.py:11
  133.8 0.3 reduce_sum.91
  134.1 1.0 copy.78
  135.1 13.3 %all-to-all-done.4 = bf16[4,2048,64]{1,2,0:T(8,128)(2,1)S(1)} async-done(((bf16[4,2048,64]{1,2,0:T(8,128)(2,1)}), bf16[4,2048,64]{1,2,0:T(8,128)(2,1)S(1)}, u32[]{:S(2)}, u32[]{:S(2)}) %all-to-all-start.4) | async-done | bytes 1048608 | tf_op jit(solution)/shard_map/all_to_all | solution.py:11
  148.4 10.6 %all-to-all-start.3 = ((bf16[128,2,512]{2,1,0:T(2,128)(2,1)}), bf16[128,2,512]{2,1,0:T(2,128)(2,1)S(1)}, u32[]{:S(2)}, u32[]{:S(2)}) async-start(bf16[128,2,512]{2,1,0:T(2,128)(2,1)} %copy.78), calls=%async_computation.3 | async-start | bytes 524288 | tf_op jit(solution)/shard_map/all_to_all | solution.py:132
  159.0 0.2 convert_reduce_fusion
  159.3 0.3 copy.79
  159.5 1.0 reshape.244
  160.6 13.8 %all-to-all-done.3 = bf16[128,2,512]{2,1,0:T(2,128)(2,1)S(1)} async-done(((bf16[128,2,512]{2,1,0:T(2,128)(2,1)}), bf16[128,2,512]{2,1,0:T(2,128)(2,1)S(1)}, u32[]{:S(2)}, u32[]{:S(2)}) %all-to-all-start.3) | async-done | bytes 262176 | tf_op jit(solution)/shard_map/all_to_all | solution.py:132
  174.4 5.5 %all-to-all-start.5 = ((bf16[128,2,256]{2,1,0:T(2,128)(2,1)}), bf16[128,2,256]{2,1,0:T(2,128)(2,1)S(1)}, u32[]{:S(2)}, u32[]{:S(2)}) async-start(bf16[128,2,256]{2,1,0:T(2,128)(2,1)} %reshape.244), calls=%async_computation.5 | async-start | bytes 262144 | tf_op jit(solution)/shard_map/all_to_all | solution.py:147
  180.0 0.1 fusion.8
  180.1 0.1 reshape.232
  180.3 12.4 %all-to-all-done.5 = bf16[128,2,256]{2,1,0:T(2,128)(2,1)S(1)} async-done(((bf16[128,2,256]{2,1,0:T(2,128)(2,1)}), bf16[128,2,256]{2,1,0:T(2,128)(2,1)S(1)}, u32[]{:S(2)}, u32[]{:S(2)}) %all-to-all-start.5) | async-done | bytes 131104 | tf_op jit(solution)/shard_map/all_to_all | solution.py:147
  192.7 0.3 reshape.245
  193.0 0.1 copy.80
  193.1 0.5 all_to_all.37
  193.7 20.5 %all-gather.5.cloned.1.call-done = bf16[4096,512]{1,0:T(8,128)(2,1)} async-done(((bf16[32,512]{1,0:T(8,128)(2,1)}), bf16[4096,512]{1,0:T(8,128)(2,1)}) %all-gather.5.cloned.1.call-update) | async-done | bytes 4194320 | tf_op jit(solution)/shard_map/all_gather | solution.py:150
  214.1 2.8 %convolution_multiply_fusion = f32[16,512]{1,0:T(8,128)S(1)} fusion(bf16[16,4096]{1,0:T(8,128)(2,1)S(1)} %all_to_all.37, bf16[4096,512]{1,0:T(8,128)(2,1)} %all-gather.5.cloned.1.call-done, f32[16]{0:T(128)S(1)} %fusion.8), kind=kOutput, calls=%fused_computation.12 | convolution fusion | flops 67117056 | bytes 4358208 | tf_op jit(solution)/shard_map/dot_general | solution.py:148
  216.9 0.8 fusion.4
  (49 shorter events, 1.1 us)
Async XLA Ops:
  6.5 74.1 %copy-start = (bf16[1,128,2048]{2,1,0:T(8,128)(2,1)S(1)}, bf16[1,128,2048]{2,1,0:T(8,128)(2,1)}, u32[]{:S(2)}) copy-start(bf16[1,128,2048]{2,1,0:T(8,128)(2,1)} %param.37) | copy-start | bytes 1572868
  6.5 6.3 %copy-start.2 = (f32[16,1,128,128]{3,2,1,0:T(8,128)S(1)}, f32[16,1,128,128]{3,2,1,0:T(8,128)}, u32[]{:S(2)}) copy-start(f32[16,1,128,128]{3,2,1,0:T(8,128)} %param.22) | copy-start | bytes 3145732
  6.5 6.9 %copy-start.4 = (bf16[128,2048]{1,0:T(8,128)(2,1)S(1)}, bf16[128,2048]{1,0:T(8,128)(2,1)}, u32[]{:S(2)}) copy-start(bf16[128,2048]{1,0:T(8,128)(2,1)} %param.27) | copy-start | bytes 1572868
  9.7 15.1 %copy-start.1 = (bf16[16,2048]{1,0:T(8,128)(2,1)S(1)}, bf16[16,2048]{1,0:T(8,128)(2,1)}, u32[]{:S(2)}) copy-start(bf16[16,2048]{1,0:T(8,128)(2,1)} %param.20) | copy-start | bytes 196612
  11.0 13.9 %copy-start.11 = (f32[2048]{0:T(1024)S(1)}, f32[2048]{0:T(1024)}, u32[]{:S(2)}) copy-start(f32[2048]{0:T(1024)} %param.28) | copy-start | bytes 24580
  11.1 15.4 %copy-start.9 = (s32[16,6]{0,1:T(8,128)S(1)}, s32[16,6]{0,1:T(8,128)}, u32[]{:S(2)}) copy-start(s32[16,6]{0,1:T(8,128)} %param.33) | copy-start | bytes 1156
  14.4 10.4 %all-to-all-start = ((bf16[4,16,2048]{2,1,0:T(8,128)(2,1)}), bf16[4,16,2048]{2,1,0:T(8,128)(2,1)S(1)}, u32[]{:S(2)}, u32[]{:S(2)}) async-start(bf16[4,16,2048]{2,1,0:T(8,128)(2,1)} %broadcast_in_dim.13), calls=%async_computation | async-start | bytes 524288 | tf_op jit(solution)/shard_map/all_to_all | solution.py:11
  19.2 107.2 %all-gather.3.cloned.1.call-start = ((), (), s32[]{:S(2)}) async-start(), calls=%async_computation.6 | async-start | bytes 2113536 | tf_op jit(solution)/shard_map/all_gather | solution.py:137
  25.0 2.3 %copy-start.5 = (bf16[16,2048]{1,0:T(8,128)(2,1)}, bf16[16,2048]{1,0:T(8,128)(2,1)S(1)}, u32[]{:S(2)}) copy-start(bf16[16,2048]{1,0:T(8,128)(2,1)S(1)} %multiply_convert_fusion) | copy-start | bytes 196612
  25.7 188.4 %all-gather.5.cloned.1.call-start = ((), (), s32[]{:S(2)}) async-start(), calls=%async_computation.7 | async-start | bytes 4227072 | tf_op jit(solution)/shard_map/all_gather | solution.py:150
  28.5 52.1 %copy-start.3 = (bf16[1,2048,128]{2,1,0:T(8,128)(2,1)S(1)}, bf16[1,2048,128]{2,1,0:T(8,128)(2,1)}, u32[]{:S(2)}) copy-start(bf16[1,2048,128]{2,1,0:T(8,128)(2,1)} %param.36) | copy-start | bytes 1572868
  81.8 44.6 %copy-start.7 = (bf16[512,32]{0,1:T(8,128)(2,1)S(1)}, bf16[512,32]{0,1:T(8,128)(2,1)}, u32[]{:S(2)}) copy-start(bf16[512,32]{0,1:T(8,128)(2,1)} %param.31) | copy-start | bytes 98308
  81.8 44.6 %copy-start.8 = (bf16[512,32]{0,1:T(8,128)(2,1)S(1)}, bf16[512,32]{0,1:T(8,128)(2,1)}, u32[]{:S(2)}) copy-start(bf16[512,32]{0,1:T(8,128)(2,1)} %param.30) | copy-start | bytes 98308
  82.9 45.8 %all-to-all-start.2 = ((bf16[128,1,2,4,512]{4,0,2,1,3:T(8,128)(2,1)}), bf16[128,1,2,4,512]{4,0,2,1,3:T(8,128)(2,1)S(1)}, u32[]{:S(2)}, u32[]{:S(2)}) async-start(bf16[128,1,2,4,512]{4,0,2,1,3:T(8,128)(2,1)} %bitcast.91), calls=%async_computation.2 | async-start | bytes 2097152 | tf_op jit(solution)/shard_map/all_to_all | solution.py:129
  128.7 5.1 %copy-start.10 = (f32[16,6]{0,1:T(8,128)S(1)}, f32[16,6]{0,1:T(8,128)}, u32[]{:S(2)}) copy-start(f32[16,6]{0,1:T(8,128)} %param.34) | copy-start | bytes 1156
  129.9 18.6 %all-to-all-start.4 = ((bf16[4,2048,64]{1,2,0:T(8,128)(2,1)}), bf16[4,2048,64]{1,2,0:T(8,128)(2,1)S(1)}, u32[]{:S(2)}, u32[]{:S(2)}) async-start(bf16[4,2048,64]{1,2,0:T(8,128)(2,1)} %broadcast_in_dim.16), calls=%async_computation.4 | async-start | bytes 2097152 | tf_op jit(solution)/shard_map/all_to_all | solution.py:11
  135.1 44.9 %copy-start.12 = (bf16[2048]{0:T(1024)(128)(2,1)S(1)}, bf16[2048]{0:T(1024)(128)(2,1)}, u32[]{:S(2)}) copy-start(bf16[2048]{0:T(1024)(128)(2,1)} %param.29) | copy-start | bytes 12292
  135.1 44.9 %copy-start.6 = (bf16[16,2048]{1,0:T(8,128)(2,1)S(1)}, bf16[16,2048]{1,0:T(8,128)(2,1)}, u32[]{:S(2)}) copy-start(bf16[16,2048]{1,0:T(8,128)(2,1)} %copy-done.5) | copy-start | bytes 196612
  148.4 25.9 %all-to-all-start.3 = ((bf16[128,2,512]{2,1,0:T(2,128)(2,1)}), bf16[128,2,512]{2,1,0:T(2,128)(2,1)S(1)}, u32[]{:S(2)}, u32[]{:S(2)}) async-start(bf16[128,2,512]{2,1,0:T(2,128)(2,1)} %copy.78), calls=%async_computation.3 | async-start | bytes 524288 | tf_op jit(solution)/shard_map/all_to_all | solution.py:132
  174.4 18.3 %all-to-all-start.5 = ((bf16[128,2,256]{2,1,0:T(2,128)(2,1)}), bf16[128,2,256]{2,1,0:T(2,128)(2,1)S(1)}, u32[]{:S(2)}, u32[]{:S(2)}) async-start(bf16[128,2,256]{2,1,0:T(2,128)(2,1)} %reshape.244), calls=%async_computation.5 | async-start | bytes 262144 | tf_op jit(solution)/shard_map/all_to_all | solution.py:147
Sparse Core Ops, SparseCore 0:
  25.8 100.5 all-gather.2
  129.5 84.5 all-gather.4
where the time goes:
time: 225 us
  waiting for transfers between devices  106 us (47%)
  blocking collectives  50.3 us (22%)
  starting transfers between devices  28.4 us (13%)
  matrix products  14.1 us (6%)
  between operations  13.8 us (6%)
  local copies, waits for them, and re-layouts  8.01 us (4%)
  other arithmetic  3.66 us (2%)
    all_to_all x1, blocking collectives, on_device(): lax.all_to_all(packed, 'ep', split_axis=0, concat_axis=0, tiled=True)  50.3 us
    all_gather x1, waiting for transfers between devices, on_device(): lax.all_gather(own_cols, 'ep', axis=0, tiled=True)  40 us
    all_gather x1, waiting for transfers between devices, on_device(): lax.all_gather(dense_down, 'ep', axis=0, tiled=True)  20.5 us
    all_to_all x2, waiting for transfers between devices, from_everyone(): return lax.all_to_all(copies, axis, split_axis=0, concat_axis=0, tiled=True)  18.9 us
    all_to_all x1, waiting for transfers between devices, on_device(): lax.all_to_all(mine, 'ep', split_axis=0, concat_axis=0, tiled=True)  13.8 us
    all_to_all x1, waiting for transfers between devices, on_device(): lax.all_to_all(dense_hidden, 'ep', split_axis=0, concat_axis=1, tiled=True)  12.4 us
    all_to_all x1, starting transfers between devices, on_device(): lax.all_to_all(mine, 'ep', split_axis=0, concat_axis=0, tiled=True)  10.6 us
    all_to_all x2, starting transfers between devices, from_everyone(): return lax.all_to_all(copies, axis, split_axis=0, concat_axis=0, tiled=True)  8.8 us
  transfers between devices with their start and end apart: 7, of which 6 were waited for; matrix products, arithmetic and copies ran while one was open for 6% of the time, Pallas kernels for 0%

commit v1 on v0

--- a/solution.py
+++ b/solution.py
@@ -1,9 +1,63 @@
+import functools
+
 import jax
 import jax.numpy as jnp
 from jax import lax
+from jax.experimental import pallas as pl
+from jax.experimental.pallas import tpu as pltpu
 from jax.sharding import PartitionSpec as P
 
 EPS = 1e-06
+
+
+MESH = pl.DeviceIdType.MESH
+
+
+def trade_kernel(n, src, dst, send_sem, recv_sem):
+    me = lax.axis_index("ep")
+    row = lax.axis_index("tp")
+    barrier = pltpu.get_barrier_semaphore()
+
+    def greet(step, carry):
+        pl.semaphore_signal(
+            barrier, 1, device_id=(lax.rem(me + step, n), row), device_id_type=MESH
+        )
+        return carry
+
+    lax.fori_loop(1, n, greet, 0)
+    pl.semaphore_wait(barrier, n - 1)
+
+    def send(step, carry):
+        to = lax.rem(me + step, n)
+        pltpu.make_async_remote_copy(
+            src_ref=src.at[to],
+            dst_ref=dst.at[me],
+            send_sem=send_sem,
+            recv_sem=recv_sem,
+            device_id=(to, row),
+            device_id_type=MESH,
+        ).start()
+        return carry
+
+    lax.fori_loop(1, n, send, 0)
+    dst[me] = src[me]
+    most = pl.ds(0, n - 1)
+    pltpu.make_async_copy(src.at[most], dst.at[most], send_sem).wait()
+    pltpu.make_async_copy(src.at[most], dst.at[most], recv_sem).wait()
+
+
+def trade(blocks, number):
+    n = blocks.shape[0]
+    flat = blocks.reshape(n, -1, 128)
+    return pl.pallas_call(
+        functools.partial(trade_kernel, n),
+        name="trade",
+        out_shape=jax.ShapeDtypeStruct(flat.shape, flat.dtype),
+        in_specs=[pl.BlockSpec(memory_space=pltpu.VMEM)],
+        out_specs=pl.BlockSpec(memory_space=pltpu.VMEM),
+        scratch_shapes=[pltpu.SemaphoreType.DMA, pltpu.SemaphoreType.DMA],
+        compiler_params=pltpu.CompilerParams(collective_id=number, has_side_effects=True),
+    )(flat).reshape(blocks.shape)
 
 
 def from_everyone(shard, axis):
@@ -112,7 +166,7 @@
     combining = jnp.sum(jnp.where(matches, route_weights[None], 0.0), axis=2).T
     packed = jnp.dot(placing, ffn_in, preferred_element_type=jnp.float32).astype(jnp.bfloat16)
     packed = packed.reshape(experts, capacity, ffn_in.shape[1])
-    received = lax.all_to_all(packed, "ep", split_axis=0, concat_axis=0, tiled=True)
+    received = trade(packed, 0)
     count = received.shape[1]
     grouped = received.reshape(ep_count, per_device, count, model_width)
     gate_pre = jnp.einsum(
@@ -129,7 +183,7 @@
     traded = lax.all_to_all(blocks_out, "tp", split_axis=3, concat_axis=3, tiled=True)
     mine = jnp.sum(traded.astype(jnp.float32), axis=3).astype(jnp.bfloat16)
     mine = mine.reshape(ep_count * per_device, count, columns)
-    returned = lax.all_to_all(mine, "ep", split_axis=0, concat_axis=0, tiled=True)
+    returned = trade(mine, 1)
     experts_out = jnp.dot(combining, returned.reshape(slot_count, columns).astype(jnp.float32))
     hidden_units = dense_gate.shape[1]
     both_weights = jnp.concatenate([dense_gate, dense_up], axis=1)

time: 225 us -> 246 us (1.093)
  Pallas kernels: 0 us -> 70.3 us
  blocking collectives: 50.3 us -> 0 us
  local copies, waits for them, and re-layouts: 8.01 us -> 11.2 us
    pallas_call x0 -> x2, Pallas kernels: none -> 70.3 us  [trade(): pl.pallas_call(functools.partial(trade_kernel, n), name='trade', out_shap...]
    all_to_all x1 -> x0, blocking collectives: 50.3 us -> none  [on_device(): lax.all_to_all(packed, 'ep', split_axis=0, concat_axis=0, tiled=True)]
    all_gather x1, waiting for transfers between devices: 40 us -> 86.3 us  [on_device(): lax.all_gather(own_cols, 'ep', axis=0, tiled=True)]
    all_gather x1, waiting for transfers between devices: 20.5 us -> 0.02 us  [on_device(): lax.all_gather(dense_down, 'ep', axis=0, tiled=True)]
    all_to_all x1 -> x0, waiting for transfers between devices: 13.8 us -> none  [on_device(): lax.all_to_all(mine, 'ep', split_axis=0, concat_axis=0, tiled=True)]
    all_to_all x2, waiting for transfers between devices: 18.9 us -> 5.53 us  [from_everyone(): return lax.all_to_all(copies, axis, split_axis=0, concat_axis=0, tiled=True)]
    all_to_all x1, waiting for transfers between devices: 12.4 us -> 0.01 us  [on_device(): lax.all_to_all(dense_hidden, 'ep', split_axis=0, concat_axis=1, tiled=True)]
    all_to_all x1, waiting for transfers between devices: 0.01 us -> 11.8 us  [on_device(): lax.all_to_all(blocks_out, 'tp', split_axis=3, concat_axis=3, tiled=True)]
  transfers between devices with their start and end apart: 7 -> 6, of which waited for: 6 -> 3; matrix products, arithmetic and copies ran while one was open for 6% -> 7% of each run, Pallas kernels for 0% -> 29%
where the time goes in v1:
time: 246 us; the launch traced here: 245 us
  waiting for transfers between devices  104 us (42%)
  Pallas kernels  70.3 us (29%)
  starting transfers between devices  27.3 us (11%)
  between operations  13.8 us (6%)
  matrix products  13.1 us (5%)
  local copies, waits for them, and re-layouts  11.2 us (5%)
  other arithmetic  4.92 us (2%)
    all_gather x1, waiting for transfers between devices, on_device(): lax.all_gather(own_cols, 'ep', axis=0, tiled=True)  86.3 us
    pallas_call x2, Pallas kernels, trade(): pl.pallas_call(functools.partial(trade_kernel, n), name='trade', out_shap...  70.3 us
    all_to_all x1, starting transfers between devices, on_device(): lax.all_to_all(dense_hidden, 'ep', split_axis=0, concat_axis=1, tiled=True)  14.7 us
    all_to_all x1, waiting for transfers between devices, on_device(): lax.all_to_all(blocks_out, 'tp', split_axis=3, concat_axis=3, tiled=True)  11.8 us
    all_to_all x2, starting transfers between devices, from_everyone(): return lax.all_to_all(copies, axis, split_axis=0, concat_axis=0, tiled=True)  9.06 us
    all_to_all x2, waiting for transfers between devices, from_everyone(): return lax.all_to_all(copies, axis, split_axis=0, concat_axis=0, tiled=True)  5.53 us
  transfers between devices with their start and end apart: 6, of which 3 were waited for; matrix products, arithmetic and copies ran while one was open for 7% of the time, Pallas kernels for 29%

profile of v1, /device:TPU:1, one launch (start us, length us, event | category | flops | bytes accessed | tf_op | source)
XLA Modules:
  0.0 245.0 jit_solution(17600458808627371264)
XLA Ops:
  6.6 1.1 fusion.26
  7.7 0.7 convert_element_type.71
  8.3 1.3 convolution_bitcast_fusion.2
  9.7 1.4 convolution_bitcast_fusion.3
  11.1 1.3 fusion.58
  12.5 0.1 fusion.51
  12.9 0.4 fusion.9
  13.3 0.1 multiply_reduce_fusion.1
  13.4 0.2 convolution_convert_fusion.3
  13.7 0.7 broadcast_in_dim.13
  14.4 4.8 %all-to-all-start = ((bf16[4,16,2048]{2,1,0:T(8,128)(2,1)}), bf16[4,16,2048]{2,1,0:T(8,128)(2,1)S(1)}, u32[]{:S(2)}, u32[]{:S(2)}) async-start(bf16[4,16,2048]{2,1,0:T(8,128)(2,1)} %broadcast_in_dim.13), calls=%async_computation | async-start | bytes 524288 | tf_op jit(solution)/shard_map/all_to_all | solution.py:65
  19.2 5.5 %all-to-all-done = bf16[4,16,2048]{2,1,0:T(8,128)(2,1)S(1)} async-done(((bf16[4,16,2048]{2,1,0:T(8,128)(2,1)}), bf16[4,16,2048]{2,1,0:T(8,128)(2,1)S(1)}, u32[]{:S(2)}, u32[]{:S(2)}) %all-to-all-start) | async-done | bytes 262176 | tf_op jit(solution)/shard_map/all_to_all | solution.py:65
  24.8 0.1 multiply_reduce_fusion
  25.0 0.6 constant_dynamic-slice_fusion
  25.7 0.7 all-gather.5.cloned.1.call-update
  26.5 0.1 eq.30
  26.7 0.1 reduce_window_sum.11
  26.9 0.2 select_reduce_fusion.1
  27.1 0.1 copy.68
  27.2 86.3 %all-gather.3.cloned.1.call-done = bf16[2048,512]{1,0:T(8,128)(2,1)} async-done(((bf16[16,512]{1,0:T(8,128)(2,1)}), bf16[2048,512]{1,0:T(8,128)(2,1)}) %all-gather.3.cloned.1.call-update) | async-done | bytes 2097168 | tf_op jit(solution)/shard_map/all_gather | solution.py:191
  113.6 2.3 convolution_convert_fusion.2
  115.9 1.1 broadcast_in_dim.16
  117.0 4.2 %all-to-all-start.2 = ((bf16[4,2048,64]{1,2,0:T(8,128)(2,1)}), bf16[4,2048,64]{1,2,0:T(8,128)(2,1)}, u32[]{:S(2)}, u32[]{:S(2)}) async-start(bf16[4,2048,64]{1,2,0:T(8,128)(2,1)} %broadcast_in_dim.16), calls=%async_computation.2 | async-start | bytes 2097152 | tf_op jit(solution)/shard_map/all_to_all | solution.py:65
  121.4 0.5 convolution_convert_fusion.1
  121.9 1.3 reshape_reshape.10.src
  123.2 48.4 %trade.2 = bf16[128,32,128]{2,1,0:T(8,128)(2,1)} custom-call(bf16[128,32,128]{2,1,0:T(8,128)(2,1)} %reshape_reshape.10.src), custom_call_target="tpu_custom_call" | custom-call | tf_op jit(solution)/shard_map/trade/pallas_call | solution.py:52
  171.6 1.4 reshape.220
  173.0 0.7 convolution_bitcast_fusion.1
  173.8 1.1 convolution_convert_fusion
  174.9 1.1 copy.87
  176.0 3.5 %all-to-all-start.1 = ((bf16[128,1,2,4,512]{4,0,2,1,3:T(8,128)(2,1)}), bf16[128,1,2,4,512]{4,0,2,1,3:T(8,128)(2,1)S(1)}, u32[]{:S(2)}, u32[]{:S(2)}) async-start(bf16[128,1,2,4,512]{4,0,2,1,3:T(8,128)(2,1)} %bitcast.91), calls=%async_computation.1 | async-start | bytes 2097152 | tf_op jit(solution)/shard_map/all_to_all | solution.py:183
  179.5 1.4 convert_reduce_fusion
  181.1 0.3 copy.74
  181.3 1.0 reshape.237
  182.4 11.8 %all-to-all-done.1 = bf16[128,1,2,4,512]{4,0,2,1,3:T(8,128)(2,1)S(1)} async-done(((bf16[128,1,2,4,512]{4,0,2,1,3:T(8,128)(2,1)}), bf16[128,1,2,4,512]{4,0,2,1,3:T(8,128)(2,1)S(1)}, u32[]{:S(2)}, u32[]{:S(2)}) %all-to-all-start.1) | async-done | bytes 1048608 | tf_op jit(solution)/shard_map/all_to_all | solution.py:183
  194.1 14.7 %all-to-all-start.3 = ((bf16[128,2,256]{2,1,0:T(2,128)(2,1)}), bf16[128,2,256]{2,1,0:T(2,128)(2,1)S(1)}, u32[]{:S(2)}, u32[]{:S(2)}) async-start(bf16[128,2,256]{2,1,0:T(2,128)(2,1)} %reshape.237), calls=%async_computation.3 | async-start | bytes 262144 | tf_op jit(solution)/shard_map/all_to_all | solution.py:201
  208.8 0.1 select_reduce_fusion
  208.9 0.1 fusion.8
  209.1 0.3 reduce_sum.91
  209.4 0.3 copy.73
  209.6 0.9 reshape_reshape.11.src
  210.5 21.9 %trade.3 = bf16[128,8,128]{2,1,0:T(8,128)(2,1)} custom-call(bf16[128,8,128]{2,1,0:T(8,128)(2,1)} %reshape_reshape.11.src), custom_call_target="tpu_custom_call" | custom-call | tf_op jit(solution)/shard_map/trade/pallas_call | solution.py:52
  232.4 1.1 reshape_reshape.12
  233.5 0.3 reshape.238
  233.8 0.1 copy.75
  234.0 0.5 all_to_all.29
  234.5 2.8 %convolution_multiply_fusion = f32[16,512]{1,0:T(8,128)S(1)} fusion(bf16[16,4096]{1,0:T(8,128)(2,1)S(1)} %all_to_all.29, bf16[4096,512]{1,0:T(8,128)(2,1)} %all-gather.5.cloned.1.call-done, f32[16]{0:T(128)S(1)} %fusion.8), kind=kOutput, calls=%fused_computation.12 | convolution fusion | flops 67117056 | bytes 4358208 | tf_op jit(solution)/shard_map/dot_general | solution.py:202
  237.3 0.8 fusion.4
  (48 shorter events, 1.0 us)
Async XLA Ops:
  6.5 167.2 %copy-start = (bf16[1,128,2048]{2,1,0:T(8,128)(2,1)S(1)}, bf16[1,128,2048]{2,1,0:T(8,128)(2,1)}, u32[]{:S(2)}) copy-start(bf16[1,128,2048]{2,1,0:T(8,128)(2,1)} %param.37) | copy-start | bytes 1572868
  6.5 6.3 %copy-start.2 = (f32[16,1,128,128]{3,2,1,0:T(8,128)S(1)}, f32[16,1,128,128]{3,2,1,0:T(8,128)}, u32[]{:S(2)}) copy-start(f32[16,1,128,128]{3,2,1,0:T(8,128)} %param.22) | copy-start | bytes 3145732
  6.5 6.9 %copy-start.4 = (bf16[128,2048]{1,0:T(8,128)(2,1)S(1)}, bf16[128,2048]{1,0:T(8,128)(2,1)}, u32[]{:S(2)}) copy-start(bf16[128,2048]{1,0:T(8,128)(2,1)} %param.27) | copy-start | bytes 1572868
  9.7 15.1 %copy-start.1 = (bf16[16,2048]{1,0:T(8,128)(2,1)S(1)}, bf16[16,2048]{1,0:T(8,128)(2,1)}, u32[]{:S(2)}) copy-start(bf16[16,2048]{1,0:T(8,128)(2,1)} %param.20) | copy-start | bytes 196612
  11.0 13.9 %copy-start.9 = (f32[2048]{0:T(1024)S(1)}, f32[2048]{0:T(1024)}, u32[]{:S(2)}) copy-start(f32[2048]{0:T(1024)} %param.28) | copy-start | bytes 24580
  11.1 15.4 %copy-start.7 = (s32[16,6]{0,1:T(8,128)S(1)}, s32[16,6]{0,1:T(8,128)}, u32[]{:S(2)}) copy-start(s32[16,6]{0,1:T(8,128)} %param.33) | copy-start | bytes 1156
  12.4 101.1 %copy-start.5 = (bf16[512,32]{0,1:T(8,128)(2,1)S(1)}, bf16[512,32]{0,1:T(8,128)(2,1)}, u32[]{:S(2)}) copy-start(bf16[512,32]{0,1:T(8,128)(2,1)} %param.31) | copy-start | bytes 98308
  12.4 101.1 %copy-start.6 = (bf16[512,32]{0,1:T(8,128)(2,1)S(1)}, bf16[512,32]{0,1:T(8,128)(2,1)}, u32[]{:S(2)}) copy-start(bf16[512,32]{0,1:T(8,128)(2,1)} %param.30) | copy-start | bytes 98308
  14.4 10.4 %all-to-all-start = ((bf16[4,16,2048]{2,1,0:T(8,128)(2,1)}), bf16[4,16,2048]{2,1,0:T(8,128)(2,1)S(1)}, u32[]{:S(2)}, u32[]{:S(2)}) async-start(bf16[4,16,2048]{2,1,0:T(8,128)(2,1)} %broadcast_in_dim.13), calls=%async_computation | async-start | bytes 524288 | tf_op jit(solution)/shard_map/all_to_all | solution.py:65
  19.2 94.3 %all-gather.3.cloned.1.call-start = ((), (), s32[]{:S(2)}) async-start(), calls=%async_computation.4 | async-start | bytes 2113536 | tf_op jit(solution)/shard_map/all_gather | solution.py:191
  25.7 208.8 %all-gather.5.cloned.1.call-start = ((), (), s32[]{:S(2)}) async-start(), calls=%async_computation.5 | async-start | bytes 4227072 | tf_op jit(solution)/shard_map/all_gather | solution.py:204
  115.9 5.5 %copy-start.8 = (f32[16,6]{0,1:T(8,128)S(1)}, f32[16,6]{0,1:T(8,128)}, u32[]{:S(2)}) copy-start(f32[16,6]{0,1:T(8,128)} %param.34) | copy-start | bytes 1156
  117.0 58.9 %all-to-all-start.2 = ((bf16[4,2048,64]{1,2,0:T(8,128)(2,1)}), bf16[4,2048,64]{1,2,0:T(8,128)(2,1)}, u32[]{:S(2)}, u32[]{:S(2)}) async-start(bf16[4,2048,64]{1,2,0:T(8,128)(2,1)} %broadcast_in_dim.16), calls=%async_computation.2 | async-start | bytes 2097152 | tf_op jit(solution)/shard_map/all_to_all | solution.py:65
  123.2 49.8 %copy-start.11 = (bf16[1,2048,128]{2,1,0:T(8,128)(2,1)S(1)}, bf16[1,2048,128]{2,1,0:T(8,128)(2,1)}, u32[]{:S(2)}) copy-start(bf16[1,2048,128]{2,1,0:T(8,128)(2,1)} %param.35) | copy-start | bytes 1572868
  171.6 2.2 copy-start.3
  176.0 18.1 %all-to-all-start.1 = ((bf16[128,1,2,4,512]{4,0,2,1,3:T(8,128)(2,1)}), bf16[128,1,2,4,512]{4,0,2,1,3:T(8,128)(2,1)S(1)}, u32[]{:S(2)}, u32[]{:S(2)}) async-start(bf16[128,1,2,4,512]{4,0,2,1,3:T(8,128)(2,1)} %bitcast.91), calls=%async_computation.1 | async-start | bytes 2097152 | tf_op jit(solution)/shard_map/all_to_all | solution.py:183
  179.5 29.4 %copy-start.10 = (bf16[2048]{0:T(1024)(128)(2,1)S(1)}, bf16[2048]{0:T(1024)(128)(2,1)}, u32[]{:S(2)}) copy-start(bf16[2048]{0:T(1024)(128)(2,1)} %param.29) | copy-start | bytes 12292
  194.1 39.4 %all-to-all-start.3 = ((bf16[128,2,256]{2,1,0:T(2,128)(2,1)}), bf16[128,2,256]{2,1,0:T(2,128)(2,1)S(1)}, u32[]{:S(2)}, u32[]{:S(2)}) async-start(bf16[128,2,256]{2,1,0:T(2,128)(2,1)} %reshape.237), calls=%async_computation.3 | async-start | bytes 262144 | tf_op jit(solution)/shard_map/all_to_all | solution.py:201
Sparse Core Ops, SparseCore 0:
  25.8 87.6 all-gather.2
  116.7 107.8 all-gather.4

commit v2 on v0

v2 whole, which is shorter than its diff:
```python
import types

import jax
import jax.numpy as jnp
import numpy as np
from jax import lax
from jax.experimental import pallas as pl
from jax.experimental.pallas import tpu as pltpu
from jax.sharding import PartitionSpec as P

EPS = 1e-06
MESH = pl.DeviceIdType.MESH
F32 = jnp.float32
BF16 = jnp.bfloat16
NZ, NY, NC, NT = 8, 8, 2, 4
ROWS = 16
WIDTH = 2048
HEAD = 128
COLS = WIDTH // NT
HID = 128
DH = 32
NE = NZ * NC
ORDER = (0, 1, 7, 2, 6, 3, 5, 4)
CHUNKS = ((0, 3), (3, 5), (5, 8))

def dot(a, b):
    return jnp.dot(a, b, preferred_element_type=F32)


def dot_nt(a, b):
    return lax.dot_general(a, b, (((1,), (1,)), ((), ())), preferred_element_type=F32)


def dot_tn(a, b):
    return lax.dot_general(a, b, (((0,), (0,)), ((), ())), preferred_element_type=F32)


def scratch_table():
    dma = pltpu.SemaphoreType.DMA
    nch = len(CHUNKS)
    return dict(
        tok=pltpu.VMEM((ROWS, WIDTH), BF16),
        pos=pltpu.VMEM((1, ROWS), jnp.int32),
        state=pltpu.VMEM((ROWS, HEAD, HEAD), F32),
        mixg=pltpu.VMEM((WIDTH // 128, 128), F32),
        wqkv=pltpu.VMEM((WIDTH, 3 * HEAD), BF16),
        wout=pltpu.VMEM((HEAD, WIDTH), BF16),
        ffng=pltpu.VMEM((WIDTH // 128, 128), F32),
        bgate=pltpu.VMEM((WIDTH // 128, 128), BF16),
        freq=pltpu.VMEM((1, 128), F32),
        ret=pltpu.VMEM((ROWS, HEAD), F32),
        hp=pltpu.VMEM((NT, ROWS, WIDTH), BF16),
        after=pltpu.VMEM((ROWS, WIDTH), F32),
        ffn=pltpu.VMEM((ROWS, WIDTH), BF16),
        x=pltpu.VMEM((NY, ROWS, COLS), BF16),
        rt=pltpu.VMEM((NY, 6, ROWS), jnp.int32),
        sc=pltpu.VMEM((NY, 6, ROWS), F32),
        bw=pltpu.VMEM((NY, ROWS, 128), F32),
        place=pltpu.VMEM((NE * ROWS, 128), BF16),
        weigh=pltpu.VMEM((NE * ROWS, 128), BF16),
        slots=pltpu.VMEM((NE, ROWS, COLS), BF16),
        got=pltpu.VMEM((NE, ROWS, COLS), BF16),
        wgu=pltpu.VMEM((NT, COLS, 2 * HID), BF16),
        wdn=pltpu.VMEM((NT, HID, COLS), BF16),
        part=pltpu.VMEM((NT, NE * ROWS, 2 * HID), BF16),
        parts=pltpu.VMEM((NT, NE * ROWS, 2 * HID), BF16),
        hid=pltpu.VMEM((NE * ROWS, HID), BF16),
        hids=pltpu.VMEM((NE * ROWS, NT * HID), BF16),
        rows=pltpu.VMEM((NE, ROWS, COLS), BF16),
        back=pltpu.VMEM((NE, ROWS, COLS), BF16),
        dg=pltpu.VMEM((NC, NZ, DH, COLS), BF16),
        du=pltpu.VMEM((NC, NZ, DH, COLS), BF16),
        dd=pltpu.VMEM((NC, NZ, DH, COLS), BF16),
        dpart=pltpu.VMEM((2, NY * ROWS, NE * DH), BF16),
        dparts=pltpu.VMEM((NT, 2, NY * ROWS // NT, NE * DH), BF16),
        dhid=pltpu.VMEM((NY * ROWS // NT, NE * DH), BF16),
        dhids=pltpu.VMEM((NY * ROWS, NE * DH), BF16),
        acc=pltpu.VMEM((NY, ROWS, COLS), BF16),
        fin=pltpu.VMEM((NY, ROWS, COLS), BF16),
        loc=dma((24,)),
        s_hp=dma,
        r_hp=dma,
        s_wgu=dma,
        r_wgu=dma,
        s_wdn=dma,
        r_wdn=dma,
        s_rt=dma,
        r_rt=dma,
        s_sc=dma,
        r_sc=dma,
        s_x=dma,
        r_x=dma,
        s_bw=dma,
        r_bw=dma,
        s_dw=dma((3,)),
        r_dw=dma((3,)),
        s_df=dma((3,)),
        r_df=dma((3,)),
        s_z=dma,
        r_z=dma((nch,)),
        s_rs=dma((nch,)),
        r_rs=dma((nch,)),
        s_ag=dma((nch,)),
        r_ag=dma((nch,)),
        s_rz=dma,
        r_rz=dma,
        s_drs=dma,
        r_drs=dma,
        s_dag=dma,
        r_dag=dma,
        s_y=dma,
        r_y=dma,
    )


def kernel(
    tokens,
    positions,
    state,
    mix_gain,
    w_query,
    w_key,
    w_value,
    w_out,
    ffn_gain,
    branch_gate,
    dense_gate,
    dense_up,
    dense_down,
    routes,
    scores,
    expert_gate,
    expert_up,
    expert_down,
    freq,
    out,
    *scratch,
):
    m = types.SimpleNamespace(**dict(zip(scratch_table(), scratch)))
    ep = lax.axis_index("ep")
    t = lax.axis_index("tp")
    z, y, c = ep // 16, (ep // 2) % 8, ep % 2

    def at(dz=0, dy=0, dc=0, dt=0):
        where = lax.rem(z + dz, NZ) * 16 + lax.rem(y + dy, NY) * 2 + lax.rem(c + dc, NC)
        return (where, lax.rem(t + dt, NT))

    def send(src, dst, s, r, dev):
        pltpu.make_async_remote_copy(
            src_ref=src, dst_ref=dst, send_sem=s, recv_sem=r, device_id=dev, device_id_type=MESH
        ).start()

    def wait(ref, sem):
        pltpu.make_async_copy(ref, ref, sem).wait()

    count = [0]

    def fetch(src, dst):
        copy = pltpu.make_async_copy(src, dst, m.loc.at[count[0]])
        count[0] += 1
        copy.start()
        return copy

    first = [
        fetch(tokens, m.tok),
        fetch(mix_gain, m.mixg),
    ]
    qkv = [
        fetch(n, m.wqkv.at[:, pl.ds(HEAD * k, HEAD)])
        for k, n in enumerate((w_query, w_key, w_value))
    ]
    turn = [fetch(positions, m.pos), fetch(freq, m.freq)]
    states = fetch(state, m.state)
    outs = fetch(w_out, m.wout)
    gains = [fetch(ffn_gain, m.ffng), fetch(branch_gate, m.bgate)]
    mine = pl.ds(pl.multiple_of(t * COLS, COLS), COLS)
    own = [
        fetch(routes, m.rt.at[0]),
        fetch(scores, m.sc.at[0]),
        fetch(expert_gate.at[mine], m.wgu.at[0, :, pl.ds(0, HID)]),
        fetch(expert_up.at[mine], m.wgu.at[0, :, pl.ds(HID, HID)]),
        fetch(expert_down.at[:, mine], m.wdn.at[0]),
        fetch(dense_gate, m.dg.at[0, 0]),
        fetch(dense_up, m.du.at[0, 0]),
        fetch(dense_down, m.dd.at[0, 0]),
    ]

    barrier = pltpu.get_barrier_semaphore()
    peers = (
        [at(dt=d) for d in range(1, NT)]
        + [at(dy=d) for d in range(1, NY)]
        + [at(dz=d, dc=e) for d in range(NZ) for e in range(NC) if d or e]
    )
    for dev in peers:
        pl.semaphore_signal(barrier, 1, device_id=dev, device_id_type=MESH)

    for copy in first:
        copy.wait()
    tok = m.tok[...].astype(F32)
    scale = lax.rsqrt(jnp.mean(tok * tok, axis=1, keepdims=True) + EPS)
    gain = m.mixg[...]
    normed = jnp.concatenate(
        [
            (tok[:, 128 * j : 128 * j + 128] * scale * gain[j : j + 1]).astype(BF16)
            for j in range(WIDTH // 128)
        ],
        axis=1,
    )
    for copy in turn:
        copy.wait()
    eye = lax.broadcasted_iota(jnp.int32, (ROWS, ROWS), 0) == lax.broadcasted_iota(
        jnp.int32, (ROWS, ROWS), 1
    )
    where = jnp.sum(
        jnp.where(eye, m.pos[...].astype(F32), 0.0), axis=1, keepdims=True
    )
    angle = where * m.freq[...]
    lane = lax.broadcasted_iota(jnp.int32, (ROWS, HEAD), 1)
    cosine = jnp.cos(angle)
    sine = jnp.where(lane < HEAD // 2, -jnp.sin(angle), jnp.sin(angle))
    for copy in qkv:
        copy.wait()
    qkv = dot(normed, m.wqkv[...])
    query, key, value = (qkv[:, HEAD * k : HEAD * (k + 1)] for k in range(3))

    def rotate(v):
        return v * cosine + pltpu.roll(v, HEAD // 2, 1) * sine

    query = rotate(query)
    key = rotate(key) * HEAD**-0.5
    head = t.astype(F32)
    decay = 1.0 - jnp.exp2(jnp.full((1, HEAD), -5.0 - 5.0 * head / (NT - 1), F32))
    columns = query.T
    states.wait()
    for s in range(ROWS):
        m.ret[pl.ds(s, 1), :] = jnp.sum(
            m.state[s] * columns[:, s : s + 1], axis=0, keepdims=True
        )
    retrieved = m.ret[...] * decay + jnp.sum(query * key, axis=1, keepdims=True) * value
    retrieved = retrieved * lax.rsqrt(
        jnp.mean(retrieved * retrieved, axis=1, keepdims=True) + EPS
    )
    outs.wait()
    m.hp[0] = dot(retrieved.astype(BF16), m.wout[...]).astype(BF16)

    pl.semaphore_wait(barrier, len(peers))

    for d in (2, 1, 3):
        send(m.hp.at[0], m.hp.at[NT - d], m.s_hp, m.r_hp, at(dt=d))
    for d in range(1, NY):
        send(routes, m.rt.at[NY - d], m.s_rt, m.r_rt, at(dy=d))
        send(scores, m.sc.at[NY - d], m.s_sc, m.r_sc, at(dy=d))
    for d in range(1, NT):
        block = pl.ds(pl.multiple_of(lax.rem(t + d, NT) * COLS, COLS), COLS)
        for k, n in enumerate((expert_gate, expert_up)):
            send(
                n.at[block],
                m.wgu.at[NT - d, :, pl.ds(HID * k, HID)],
                m.s_wgu,
                m.r_wgu,
                at(dt=d),
            )
    dense = (m.dg, m.du, m.dd)
    for k, src in enumerate((dense_gate, dense_up, dense_down)):
        for d in (4, 3, 5, 2, 6, 1, 7):
            send(src, dense[k].at[0, NZ - d], m.s_dw.at[k], m.r_dw.at[k], at(dz=d))
    for d in range(1, NT):
        block = pl.ds(pl.multiple_of(lax.rem(t + d, NT) * COLS, COLS), COLS)
        send(
            expert_down.at[:, block], m.wdn.at[NT - d], m.s_wdn, m.r_wdn, at(dt=d)
        )

    for copy in gains:
        copy.wait()
    wait(m.hp.at[pl.ds(1, NT - 1)], m.r_hp)
    after = tok
    for d in range(NT):
        after = after + m.hp[d].astype(F32)
    m.after[...] = after
    scale = lax.rsqrt(jnp.mean(after * after, axis=1, keepdims=True) + EPS)
    gain = m.ffng[...]
    gate = m.bgate[...].astype(F32)
    branch = jnp.zeros((ROWS, 128), F32)
    for j in range(WIDTH // 128):
        piece = (after[:, 128 * j : 128 * j + 128] * scale * gain[j : j + 1]).astype(BF16)
        m.ffn[:, 128 * j : 128 * j + 128] = piece
        branch = branch + piece.astype(F32) * gate[j : j + 1]
    m.x[0] = m.ffn[:, mine]
    for d in (4, 3, 5, 2, 6, 1, 7):
        send(m.x.at[0], m.x.at[NY - d], m.s_x, m.r_x, at(dy=d))
    branch = jnp.sum(branch, axis=1, keepdims=True)
    m.bw[0] = jnp.broadcast_to(1.0 / (1.0 + jnp.exp(-branch)), (ROWS, 128))
    for d in (4, 3, 5, 2, 6, 1, 7):
        send(m.bw.at[0], m.bw.at[NY - d], m.s_bw, m.r_bw, at(dy=d))

    for copy in own:
        copy.wait()
    wait(m.rt.at[pl.ds(1, NY - 1)], m.r_rt)
    wait(m.sc.at[pl.ds(1, NY - 1)], m.r_sc)
    chosen = jnp.concatenate([m.rt[d] for d in range(NY)], axis=1)
    scored = jnp.concatenate([m.sc[d] for d in range(NY)], axis=1)
    shares = scored / jnp.sum(scored, axis=0, keepdims=True)
    k = lax.broadcasted_iota(jnp.int32, (NE, 128), 0)
    lane = lax.broadcasted_iota(jnp.int32, (NE, 128), 1)
    expert = ((z + k // 2) & 7) * 16 + y * 2 + ((c + k) & 1)
    named = jnp.zeros((NE, 128), F32)
    share = jnp.zeros((NE, 128), F32)
    for n in range(6):
        hit = chosen[n : n + 1] == expert
        named = jnp.where(hit, 1.0, named)
        share = jnp.where(hit, shares[n : n + 1], share)
    a = lax.broadcasted_iota(jnp.int32, (128, 128), 0)
    b = lax.broadcasted_iota(jnp.int32, (128, 128), 1)
    ahead = jnp.where((a // ROWS == b // ROWS) & (a < b), 1.0, 0.0).astype(BF16)
    rank = dot(named.astype(BF16), ahead)
    code = jnp.where(named > 0.5, rank + (2 * (lane // ROWS)).astype(F32), -1.0)
    slot = lax.broadcasted_iota(jnp.int32, (ROWS, 128), 0).astype(F32)
    for n in range(NE):
        hit = code[n : n + 1] == slot
        m.place[pl.ds(ROWS * n, ROWS), :] = jnp.where(hit, 1.0, 0.0).astype(BF16)
        m.weigh[pl.ds(ROWS * n, ROWS), :] = jnp.where(hit, share[n : n + 1], 0.0).astype(BF16)

    wait(m.x.at[pl.ds(1, NY - 1)], m.r_x)
    x = m.x[...].reshape(NY * ROWS, COLS)
    m.slots[...] = dot(m.place[...], x).astype(BF16).reshape(NE, ROWS, COLS)
    m.got[0] = m.slots[0]

    def chunk_of(place):
        return [n for n, (lo, hi) in enumerate(CHUNKS) if lo <= place < hi][0]

    for d in ORDER:
        place = ORDER.index((NZ - d) % NZ)
        for e in range(NC):
            if d or e:
                send(
                    m.slots.at[NC * d + e],
                    m.got.at[NC * place + e],
                    m.s_z,
                    m.r_z.at[chunk_of(place)],
                    at(dz=d, dc=e),
                )

    for k, n in enumerate(dense):
        wait(n.at[0, pl.ds(1, NZ - 1)], m.r_dw.at[k])
        send(n.at[0], n.at[1], m.s_df.at[k], m.r_df.at[k], at(dc=1))
    for k, n in enumerate(dense[:2]):
        wait(n.at[1], m.r_df.at[k])
        weights = n[...].reshape(NE * DH, COLS)
        m.dpart[k] = dot_nt(x, weights).astype(BF16)
    quarter = NY * ROWS // NT
    for d in (2, 1, 3):
        block = pl.ds(pl.multiple_of(lax.rem(t + d, NT) * quarter, quarter), quarter)
        send(m.dpart.at[:, block], m.dparts.at[NT - d], m.s_drs, m.r_drs, at(dt=d))
    block = pl.ds(pl.multiple_of(t * quarter, quarter), quarter)

    wait(m.wgu.at[pl.ds(1, NT - 1)], m.r_wgu)
    spans = [(lo * NC * ROWS, (hi - lo) * NC * ROWS) for lo, hi in CHUNKS]
    for n, (lo, hi) in enumerate(CHUNKS):
        start, size = spans[n]
        begin = max(NC * lo, 1)
        wait(m.got.at[pl.ds(begin, NC * hi - begin)], m.r_z.at[n])
        rows = m.got[NC * lo : NC * hi].reshape(size, COLS)
        for d in (2, 1, 3, 0):
            m.part[d, pl.ds(start, size)] = dot(rows, m.wgu[d]).astype(BF16)
            if d:
                send(
                    m.part.at[d, pl.ds(start, size)],
                    m.parts.at[NT - d, pl.ds(start, size)],
                    m.s_rs.at[n],
                    m.r_rs.at[n],
                    at(dt=d),
                )
    for n, (start, size) in enumerate(spans):
        span = pl.ds(start, size)
        wait(m.parts.at[pl.ds(1, NT - 1), span], m.r_rs.at[n])
        total = m.part[0, span].astype(F32)
        for d in range(1, NT):
            total = total + m.parts[d, span].astype(F32)
        pre = total[:, :HID]
        hidden = (pre / (1.0 + jnp.exp(-pre)) * total[:, HID:]).astype(BF16)
        m.hid[span] = hidden
        m.hids[span, 0:HID] = hidden
        for d in (2, 1, 3):
            send(
                m.hid.at[span],
                m.hids.at[span, pl.ds(HID * (NT - d), HID)],
                m.s_ag.at[n],
                m.r_ag.at[n],
                at(dt=d),
            )
    wait(m.dparts.at[pl.ds(1, NT - 1)], m.r_drs)
    pre = m.dpart[0, block].astype(F32)
    up = m.dpart[1, block].astype(F32)
    for d in range(1, NT):
        pre = pre + m.dparts[d, 0].astype(F32)
        up = up + m.dparts[d, 1].astype(F32)
    dhidden = (pre / (1.0 + jnp.exp(-pre)) * up).astype(BF16)
    m.dhid[...] = dhidden
    m.dhids[block] = dhidden
    for d in (2, 1, 3):
        send(m.dhid, m.dhids.at[block], m.s_dag, m.r_dag, at(dt=d))
    wait(m.wdn.at[pl.ds(1, NT - 1)], m.r_wdn)
    down = m.wdn[...].reshape(NT * HID, COLS)
    for n, (start, size) in enumerate(spans):
        span = pl.ds(start, size)
        lo, hi = CHUNKS[n]
        wait(m.hids.at[span, pl.ds(HID, (NT - 1) * HID)], m.r_ag.at[n])
        m.rows[NC * lo : NC * hi] = (
            dot(m.hids[span], down).astype(BF16).reshape(NC * (hi - lo), ROWS, COLS)
        )
        for place in range(lo, hi):
            d = ORDER[place]
            for e in range(NC):
                if d or e:
                    send(
                        m.rows.at[NC * place + e],
                        m.back.at[NC * ((NZ - d) % NZ) + e],
                        m.s_rz,
                        m.r_rz,
                        at(dz=d, dc=e),
                    )
    m.back[0] = m.rows[0]
    wait(m.dd.at[1], m.r_df.at[2])
    wait(m.dhids.at[pl.ds(0, NY * ROWS - quarter)], m.r_dag)
    wait(m.bw.at[pl.ds(1, NY - 1)], m.r_bw)
    extra = dot(m.dhids[...], m.dd[...].reshape(NE * DH, COLS))
    weight = m.bw[...].reshape(NY * ROWS, 128)
    extra = jnp.concatenate(
        [extra[:, 128 * j : 128 * j + 128] * weight for j in range(COLS // 128)], axis=1
    )
    wait(m.back.at[pl.ds(1, NE - 1)], m.r_rz)
    both = extra + dot_tn(m.weigh[...], m.back[...].reshape(NE * ROWS, COLS))
    m.acc[...] = both.astype(BF16).reshape(NY, ROWS, COLS)
    for d in (4, 3, 5, 2, 6, 1, 7):
        send(m.acc.at[d], m.fin.at[NY - d], m.s_y, m.r_y, at(dy=d))
    total = m.after[:, mine] + m.acc[0].astype(F32)
    wait(m.fin.at[pl.ds(1, NY - 1)], m.r_y)
    for d in range(1, NY):
        total = total + m.fin[d].astype(F32)
    out[...] = total.astype(BF16)

    wait(m.hp.at[pl.ds(1, NT - 1)], m.s_hp)
    wait(m.rt.at[pl.ds(1, NY - 1)], m.s_rt)
    wait(m.sc.at[pl.ds(1, NY - 1)], m.s_sc)
    wait(m.wgu.at[pl.ds(1, NT - 1)], m.s_wgu)
    wait(m.wdn.at[pl.ds(1, NT - 1)], m.s_wdn)
    wait(m.x.at[pl.ds(1, NY - 1)], m.s_x)
    wait(m.bw.at[pl.ds(1, NY - 1)], m.s_bw)
    for k, n in enumerate(dense):
        wait(n.at[0, pl.ds(1, NZ - 1)], m.s_dw.at[k])
        wait(n.at[1], m.s_df.at[k])
    wait(m.got.at[pl.ds(1, NE - 1)], m.s_z)
    for n, (start, size) in enumerate(spans):
        span = pl.ds(start, size)
        wait(m.parts.at[pl.ds(1, NT - 1), span], m.s_rs.at[n])
        wait(m.hids.at[span, pl.ds(HID, (NT - 1) * HID)], m.s_ag.at[n])
    wait(m.dparts.at[pl.ds(1, NT - 1)], m.s_drs)
    wait(m.dhids.at[pl.ds(0, NY * ROWS - quarter)], m.s_dag)
    wait(m.back.at[pl.ds(1, NE - 1)], m.s_rz)
    wait(m.fin.at[pl.ds(1, NY - 1)], m.s_y)


def on_device(
    tokens,
    positions,
    state,
    mix_gain,
    w_query,
    w_key,
    w_value,
    w_out,
    ffn_gain,
    branch_gate,
    dense_gate,
    dense_up,
    dense_down,
    routes,
    route_scores,
    expert_gate,
    expert_up,
    expert_down,
):
    half = HEAD // 2
    inverse = 10000.0 ** -(np.arange(half, dtype=np.float64) / (half - 1))
    freq = jnp.asarray(np.concatenate([inverse, inverse])[None], F32)
    args = (
        tokens,
        positions.reshape(1, ROWS),
        state.reshape(ROWS, HEAD, HEAD),
        mix_gain.reshape(WIDTH // 128, 128),
        w_query,
        w_key,
        w_value,
        w_out,
        ffn_gain.reshape(WIDTH // 128, 128),
        branch_gate.reshape(WIDTH // 128, 128),
        dense_gate.T,
        dense_up.T,
        dense_down,
        routes.T,
        route_scores.T,
        expert_gate.reshape(WIDTH, HID),
        expert_up.reshape(WIDTH, HID),
        expert_down.reshape(HID, WIDTH),
        freq,
    )
    return pl.pallas_call(
        kernel,
        name="layer",
        out_shape=jax.ShapeDtypeStruct((ROWS, COLS), BF16),
        in_specs=[pl.BlockSpec(memory_space=pltpu.HBM)] * len(args),
        out_specs=pl.BlockSpec(memory_space=pltpu.VMEM),
        scratch_shapes=list(scratch_table().values()),
        compiler_params=pltpu.CompilerParams(
            collective_id=0, has_side_effects=True, vmem_limit_bytes=60 * 1024 * 1024
        ),
    )(*args)


def solution(mesh):
    placed = (
        P("ep", None),
        P("ep"),
        P("ep", "tp", None, None),
        P(),
        P(None, "tp"),
        P(None, "tp"),
        P(None, "tp"),
        P("tp", None),
        P(),
        P(),
        P("tp", "ep"),
        P("tp", "ep"),
        P("ep", "tp"),
        P("ep", None),
        P("ep", None),
        P("ep", None, "tp"),
        P("ep", None, "tp"),
        P("ep", "tp", None),
    )
    return jax.shard_map(
        on_device, mesh=mesh, in_specs=placed, out_specs=P("ep", "tp"), check_vma=False
    )
```

time: 225 us -> 65.1 us (0.29)
  waiting for transfers between devices: 106 us -> 0 us
  Pallas kernels: 0 us -> 63.6 us
  blocking collectives: 50.3 us -> 0 us
  starting transfers between devices: 28.4 us -> 0 us
  matrix products: 14.1 us -> 0 us
  between operations: 13.8 us -> 0.01 us
  local copies, waits for them, and re-layouts: 8.01 us -> 1.32 us
  other arithmetic: 3.66 us -> 0 us
    pallas_call x0 -> x1, Pallas kernels: none -> 63.6 us  [on_device(): pl.pallas_call(kernel, name='layer', out_shape=jax.ShapeDtypeStruct((ROWS...]
    all_gather x2 -> x0, waiting for transfers between devices: 60.4 us -> none  [the longest x1 40 us: on_device(): lax.all_gather(own_cols, 'ep', axis=0, tiled=True)]
    all_to_all x1 -> x0, blocking collectives: 50.3 us -> none  [on_device(): lax.all_to_all(packed, 'ep', split_axis=0, concat_axis=0, tiled=True)]
    all_to_all x5 -> x0, waiting for transfers between devices: 45.1 us -> none  [the longest x2 18.9 us: from_everyone(): return lax.all_to_all(copies, axis, split_axis=0, concat_axis=0, tiled=True)]
    all_to_all x5 -> x0, starting transfers between devices: 28.4 us -> none  [the longest x1 10.6 us: on_device(): lax.all_to_all(mine, 'ep', split_axis=0, concat_axis=0, tiled=True)]
    dot_general x12 -> x0, matrix products: 14.1 us -> none  [the longest x1 2.79 us: on_device(): jnp.dot(own_hidden, lax.all_gather(dense_down, 'ep', axis=0, tiled=True),...]
  transfers between devices with their start and end apart: 7 -> 0, of which waited for: 6 -> 0; matrix products, arithmetic and copies ran while one was open for 6% -> 0% of each run, Pallas kernels for 0% -> 0%
where the time goes in v2:
time: 65.1 us; the launch traced here: 64.9 us
  Pallas kernels  63.6 us (98%)
  local copies, waits for them, and re-layouts  1.32 us (2%)
    pallas_call x1, Pallas kernels, on_device(): pl.pallas_call(kernel, name='layer', out_shape=jax.ShapeDtypeStruct((ROWS...  63.6 us
    unnamed x1, local copies, waits for them, and re-layouts  1.32 us

profile of v2, /device:TPU:1, one launch (start us, length us, event | category | flops | bytes accessed | tf_op | source)
XLA Modules:
  0.0 64.9 jit_solution(1581865291301933692)
XLA Ops:
  0.0 63.6 %layer.1 = bf16[16,512]{1,0:T(8,128)(2,1)} custom-call(bf16[16,2048]{1,0:T(8,128)(2,1)} %tokens.1, s32[1,16]{1,0:T(1,128)} %bitcast.23, f32[16,128,128]{2,1,0:T(8,128)} %bitcast.12, f32[16,128]{1,0:T(8,128)} %bitcast.18, bf16[2048,128]{1,0:T(8,128)(2,1)} %w_query.1, bf16[2048,128]{1,0:T(8,128)(2,1)} %w_key.1, bf16[2048,128]{1,0:T(8,128)(2,1)} %w_value.1, ...), custom_call_target="tpu_custom_call" | custom-call | tf_op jit(solution)/shard_map/layer/pallas_call | solution.py:507
  63.6 1.3 %copy.21 = bf16[16,512]{1,0:T(8,128)(2,1)} copy(bf16[16,512]{1,0:T(8,128)(2,1)} %layer.1) | data formatting | bytes 32768

commit v3 on v2

v3 whole, which is shorter than its diff:
```python
import types

import jax
import jax.numpy as jnp
import numpy as np
from jax import lax
from jax.experimental import pallas as pl
from jax.experimental.pallas import tpu as pltpu
from jax.sharding import PartitionSpec as P

EPS = 1e-06
MESH = pl.DeviceIdType.MESH
F32 = jnp.float32
BF16 = jnp.bfloat16
NZ, NY, NC, NT = 8, 8, 2, 4
ROWS = 16
WIDTH = 2048
HEAD = 128
COLS = WIDTH // NT
HID = 128
DH = 32
NE = NZ * NC
ORDER = (4, 3, 5, 2, 6, 1, 7, 0)
CHUNKS = ((0, 3), (3, 5), (5, 8))
FAR = (4, 3, 5, 2, 6, 1, 7)

def dot(a, b):
    return jnp.dot(a, b, preferred_element_type=F32)


def dot_nt(a, b):
    return lax.dot_general(a, b, (((1,), (1,)), ((), ())), preferred_element_type=F32)


def dot_tn(a, b):
    return lax.dot_general(a, b, (((0,), (0,)), ((), ())), preferred_element_type=F32)


def scratch_table():
    dma = pltpu.SemaphoreType.DMA
    nch = len(CHUNKS)
    gathered = NY * ROWS
    return dict(
        tok=pltpu.VMEM((ROWS, WIDTH), BF16),
        pos=pltpu.VMEM((1, ROWS), jnp.int32),
        state=pltpu.VMEM((ROWS, HEAD, HEAD), F32),
        mixg=pltpu.VMEM((WIDTH // 128, 128), F32),
        wqkv=pltpu.VMEM((WIDTH, 3 * HEAD), BF16),
        wout=pltpu.VMEM((HEAD, WIDTH), BF16),
        ffng=pltpu.VMEM((WIDTH // 128, 128), F32),
        bgate=pltpu.VMEM((WIDTH // 128, 128), BF16),
        freq=pltpu.VMEM((1, 128), F32),
        ret=pltpu.VMEM((ROWS, HEAD), F32),
        hp=pltpu.VMEM((NT, ROWS, WIDTH), BF16),
        after=pltpu.VMEM((ROWS, WIDTH), F32),
        ffn=pltpu.VMEM((ROWS, WIDTH), BF16),
        x=pltpu.VMEM((NY, ROWS, 2 * COLS), BF16),
        rt=pltpu.VMEM((NY, 6, ROWS), jnp.int32),
        sc=pltpu.VMEM((NY, 6, ROWS), F32),
        place=pltpu.VMEM((NE * ROWS, 128), BF16),
        weigh=pltpu.VMEM((NE * ROWS, 128), BF16),
        slots=pltpu.VMEM((NE, ROWS, 2 * COLS), BF16),
        got=pltpu.VMEM((NE, ROWS, WIDTH), BF16),
        wgu=pltpu.VMEM((WIDTH, 2 * HID), BF16),
        wdn=pltpu.VMEM((NT, HID, COLS), BF16),
        half=pltpu.VMEM((NE * ROWS, 2 * HID), F32),
        hid=pltpu.VMEM((NE * ROWS, HID), BF16),
        hids=pltpu.VMEM((NE * ROWS, NT * HID), BF16),
        rows=pltpu.VMEM((NE, ROWS, COLS), BF16),
        back=pltpu.VMEM((NE, ROWS, COLS), BF16),
        acc=pltpu.VMEM((NY, ROWS, COLS), BF16),
        fin=pltpu.VMEM((NY, ROWS, COLS), BF16),
        dx=pltpu.VMEM((NY, ROWS, COLS), BF16),
        dg=pltpu.VMEM((NZ, DH, COLS), BF16),
        du=pltpu.VMEM((NZ, DH, COLS), BF16),
        dd=pltpu.VMEM((NZ, DH, COLS), BF16),
        dpart=pltpu.VMEM((2, 2 * gathered, NZ * DH), BF16),
        dparts=pltpu.VMEM((NT, 2, 2 * gathered // NT, NZ * DH), BF16),
        dhid=pltpu.VMEM((2 * gathered // NT, NZ * DH), BF16),
        dhids=pltpu.VMEM((2 * gathered, NZ * DH), BF16),
        dacc=pltpu.VMEM((NC * NY, ROWS, COLS), BF16),
        dfin=pltpu.VMEM((NC * NY, ROWS, COLS), BF16),
        loc=dma((32,)),
        s_hp=dma,
        r_hp=dma,
        s_wdn=dma,
        r_wdn=dma,
        s_rt=dma,
        r_rt=dma,
        s_sc=dma,
        r_sc=dma,
        s_x=dma,
        r_x=dma,
        s_dx=dma,
        r_dx=dma,
        s_dw=dma((3,)),
        r_dw=dma((3,)),
        s_z=dma,
        r_z=dma((nch,)),
        s_up=dma((nch,)),
        r_up=dma((nch,)),
        s_ag=dma((nch,)),
        r_ag=dma((nch,)),
        s_rz=dma,
        r_rz=dma,
        s_drs=dma,
        r_drs=dma,
        s_dag=dma,
        r_dag=dma,
        s_dy=dma,
        r_dy=dma,
        s_y=dma,
        r_y=dma,
    )


def kernel(
    tokens,
    positions,
    state,
    mix_gain,
    w_query,
    w_key,
    w_value,
    w_out,
    ffn_gain,
    branch_gate,
    dense_gate,
    dense_up,
    dense_down,
    routes,
    scores,
    expert_gate,
    expert_up,
    expert_down,
    freq,
    out,
    *scratch,
):
    m = types.SimpleNamespace(**dict(zip(scratch_table(), scratch)))
    ep = lax.axis_index("ep")
    t = lax.axis_index("tp")
    z, y, c = ep // 16, (ep // 2) % 8, ep % 2

    def at(a=0, b=0, dc=0, dt=0):
        to_z = lax.rem(z + a * c + b * (1 - c), NZ)
        to_y = lax.rem(y + a * (1 - c) + b * c, NY)
        return (to_z * 16 + to_y * 2 + lax.rem(c + dc, NC), lax.rem(t + dt, NT))

    def send(src, dst, s, r, dev):
        pltpu.make_async_remote_copy(
            src_ref=src, dst_ref=dst, send_sem=s, recv_sem=r, device_id=dev, device_id_type=MESH
        ).start()

    def wait(ref, sem):
        pltpu.make_async_copy(ref, ref, sem).wait()

    def block(d):
        return pl.ds(pl.multiple_of(lax.rem(t + d, NT) * COLS, COLS), COLS)

    count = [0]

    def fetch(src, dst):
        copy = pltpu.make_async_copy(src, dst, m.loc.at[count[0]])
        count[0] += 1
        copy.start()
        return copy

    first = [fetch(tokens, m.tok), fetch(mix_gain, m.mixg)]
    qkv = [
        fetch(n, m.wqkv.at[:, pl.ds(HEAD * k, HEAD)])
        for k, n in enumerate((w_query, w_key, w_value))
    ]
    turn = [fetch(positions, m.pos), fetch(freq, m.freq)]
    states = fetch(state, m.state)
    outs = fetch(w_out, m.wout)
    gains = [fetch(ffn_gain, m.ffng), fetch(branch_gate, m.bgate)]
    own = [
        fetch(routes, m.rt.at[0]),
        fetch(scores, m.sc.at[0]),
        fetch(expert_down.at[:, block(0)], m.wdn.at[0]),
        fetch(dense_gate, m.dg.at[0]),
        fetch(dense_up, m.du.at[0]),
        fetch(dense_down, m.dd.at[0]),
    ]
    experts = [
        fetch(n.at[block(d)], m.wgu.at[pl.ds(COLS * d, COLS), pl.ds(HID * k, HID)])
        for d in range(NT)
        for k, n in enumerate((expert_gate, expert_up))
    ]

    barrier = pltpu.get_barrier_semaphore()
    peers = (
        [at(dt=d) for d in range(1, NT)]
        + [at(a=d) for d in range(1, NY)]
        + [at(b=d) for d in range(1, NY)]
        + [at(a=d, dc=1) for d in range(NY)]
        + [at(b=d, dc=1) for d in range(1, NY)]
    )
    for dev in peers:
        pl.semaphore_signal(barrier, 1, device_id=dev, device_id_type=MESH)

    for copy in first:
        copy.wait()
    tok = m.tok[...].astype(F32)
    scale = lax.rsqrt(jnp.mean(tok * tok, axis=1, keepdims=True) + EPS)
    gain = m.mixg[...]
    normed = jnp.concatenate(
        [
            (tok[:, 128 * j : 128 * j + 128] * scale * gain[j : j + 1]).astype(BF16)
            for j in range(WIDTH // 128)
        ],
        axis=1,
    )
    for copy in turn:
        copy.wait()
    eye = lax.broadcasted_iota(jnp.int32, (ROWS, ROWS), 0) == lax.broadcasted_iota(
        jnp.int32, (ROWS, ROWS), 1
    )
    where = jnp.sum(jnp.where(eye, m.pos[...].astype(F32), 0.0), axis=1, keepdims=True)
    angle = where * m.freq[...]
    lane = lax.broadcasted_iota(jnp.int32, (ROWS, HEAD), 1)
    cosine = jnp.cos(angle)
    sine = jnp.where(lane < HEAD // 2, -jnp.sin(angle), jnp.sin(angle))
    for copy in qkv:
        copy.wait()
    qkv = dot(normed, m.wqkv[...])
    query, key, value = (qkv[:, HEAD * k : HEAD * (k + 1)] for k in range(3))

    def rotate(v):
        return v * cosine + pltpu.roll(v, HEAD // 2, 1) * sine

    query = rotate(query)
    key = rotate(key) * HEAD**-0.5
    head = t.astype(F32)
    decay = 1.0 - jnp.exp2(jnp.full((1, HEAD), -5.0 - 5.0 * head / (NT - 1), F32))
    columns = query.T
    states.wait()
    for s in range(ROWS):
        m.ret[pl.ds(s, 1), :] = jnp.sum(
            m.state[s] * columns[:, s : s + 1], axis=0, keepdims=True
        )
    retrieved = m.ret[...] * decay + jnp.sum(query * key, axis=1, keepdims=True) * value
    retrieved = retrieved * lax.rsqrt(
        jnp.mean(retrieved * retrieved, axis=1, keepdims=True) + EPS
    )
    outs.wait()
    m.hp[0] = dot(retrieved.astype(BF16), m.wout[...]).astype(BF16)

    pl.semaphore_wait(barrier, len(peers))

    for d in (2, 1, 3):
        send(m.hp.at[0], m.hp.at[NT - d], m.s_hp, m.r_hp, at(dt=d))
    for d in range(1, NY):
        send(routes, m.rt.at[NY - d], m.s_rt, m.r_rt, at(a=d))
        send(scores, m.sc.at[NY - d], m.s_sc, m.r_sc, at(a=d))
    dense = (m.dg, m.du, m.dd)

    def spread(k, src):
        for d in FAR:
            send(src, dense[k].at[NZ - d], m.s_dw.at[k], m.r_dw.at[k], at(b=d))

    spread(0, dense_gate)

    for copy in gains:
        copy.wait()
    wait(m.hp.at[pl.ds(1, NT - 1)], m.r_hp)
    after = tok
    for d in range(NT):
        after = after + m.hp[d].astype(F32)
    m.after[...] = after
    scale = lax.rsqrt(jnp.mean(after * after, axis=1, keepdims=True) + EPS)
    gain = m.ffng[...]
    for j in range(WIDTH // 128):
        m.ffn[:, 128 * j : 128 * j + 128] = (
            after[:, 128 * j : 128 * j + 128] * scale * gain[j : j + 1]
        ).astype(BF16)
    for d in range(2):
        m.x[0, :, COLS * d : COLS * (d + 1)] = m.ffn[:, block(d)]
    for d in FAR:
        send(m.x.at[0], m.x.at[NY - d], m.s_x, m.r_x, at(a=d))
    for d in (2, 1, 3):
        send(expert_down.at[:, block(d)], m.wdn.at[NT - d], m.s_wdn, m.r_wdn, at(dt=d))

    for copy in own:
        copy.wait()
    wait(m.rt.at[pl.ds(1, NY - 1)], m.r_rt)
    wait(m.sc.at[pl.ds(1, NY - 1)], m.r_sc)
    chosen = jnp.concatenate([m.rt[d] for d in range(NY)], axis=1)
    scored = jnp.concatenate([m.sc[d] for d in range(NY)], axis=1)
    shares = scored / jnp.sum(scored, axis=0, keepdims=True)
    k = lax.broadcasted_iota(jnp.int32, (NE, 128), 0)
    lane = lax.broadcasted_iota(jnp.int32, (NE, 128), 1)
    expert = (
        ((z + (k // 2) * (1 - c)) & 7) * 16 + ((y + (k // 2) * c) & 7) * 2 + ((c + k) & 1)
    )
    named = jnp.zeros((NE, 128), F32)
    share = jnp.zeros((NE, 128), F32)
    for n in range(6):
        hit = chosen[n : n + 1] == expert
        named = jnp.where(hit, 1.0, named)
        share = jnp.where(hit, shares[n : n + 1], share)
    a = lax.broadcasted_iota(jnp.int32, (128, 128), 0)
    b = lax.broadcasted_iota(jnp.int32, (128, 128), 1)
    ahead = jnp.where((a // ROWS == b // ROWS) & (a < b), 1.0, 0.0).astype(BF16)
    rank = dot(named.astype(BF16), ahead)
    code = jnp.where(named > 0.5, rank + (2 * (lane // ROWS)).astype(F32), -1.0)
    slot = lax.broadcasted_iota(jnp.int32, (ROWS, 128), 0).astype(F32)
    for n in range(NE):
        hit = code[n : n + 1] == slot
        m.place[pl.ds(ROWS * n, ROWS), :] = jnp.where(hit, 1.0, 0.0).astype(BF16)
        m.weigh[pl.ds(ROWS * n, ROWS), :] = jnp.where(hit, share[n : n + 1], 0.0).astype(BF16)

    left = pl.ds(0, 2 * COLS)
    wait(m.x.at[pl.ds(1, NY - 1)], m.r_x)
    m.slots[...] = (
        dot(m.place[...], m.x[...].reshape(NY * ROWS, 2 * COLS))
        .astype(BF16)
        .reshape(NE, ROWS, 2 * COLS)
    )
    m.got[NE - NC, :, left] = m.slots[0]

    def chunk_of(spot):
        return [n for n, (lo, hi) in enumerate(CHUNKS) if lo <= spot < hi][0]

    for d in FAR + (0,):
        spot = ORDER.index((NZ - d) % NZ)
        for e in range(NC):
            if d or e:
                send(
                    m.slots.at[NC * d + e],
                    m.got.at[NC * spot + e, :, left],
                    m.s_z,
                    m.r_z.at[chunk_of(spot)],
                    at(b=d, dc=e),
                )
    for d in FAR + (0,):
        send(
            m.x.at[0, :, pl.ds(0, COLS)], m.dx.at[(NY - d) % NY], m.s_dx, m.r_dx, at(b=d, dc=1)
        )

    spread(1, dense_up)

    for copy in experts:
        copy.wait()
    spans = [(lo * NC * ROWS, (hi - lo) * NC * ROWS) for lo, hi in CHUNKS]
    for n, (lo, hi) in enumerate(CHUNKS):
        start, size = spans[n]
        some = pl.ds(NC * lo, NC * (hi - lo))
        fresh = pl.ds(NC * lo, NC * (hi - lo) - (hi == NZ))
        wait(m.got.at[fresh, :, left], m.r_z.at[n])
        for k, d in ((0, 1), (1, 3)):
            send(
                m.got.at[some, :, pl.ds(COLS * k, COLS)],
                m.got.at[some, :, pl.ds(COLS * (3 - k), COLS)],
                m.s_up.at[n],
                m.r_up.at[n],
                at(dt=d),
            )
        m.half[pl.ds(start, size)] = dot(
            m.got[NC * lo : NC * hi, :, 0 : 2 * COLS].reshape(size, 2 * COLS),
            m.wgu[0 : 2 * COLS],
        )
    spread(2, dense_down)

    wait(m.dx, m.r_dx)
    gathered = NY * ROWS
    for k in range(2):
        wait(dense[k].at[pl.ds(1, NZ - 1)], m.r_dw.at[k])
        weights = dense[k][...].reshape(NZ * DH, COLS)
        m.dpart[k, 0:gathered] = dot_nt(
            m.x[:, :, 0:COLS].reshape(gathered, COLS), weights
        ).astype(BF16)
        m.dpart[k, gathered:] = dot_nt(m.dx[...].reshape(gathered, COLS), weights).astype(BF16)
    quarter = 2 * gathered // NT

    def part(d):
        return pl.ds(pl.multiple_of(lax.rem(t + d, NT) * quarter, quarter), quarter)

    for d in (2, 1, 3):
        send(m.dpart.at[:, part(d)], m.dparts.at[NT - d], m.s_drs, m.r_drs, at(dt=d))

    for n, (lo, hi) in enumerate(CHUNKS):
        start, size = spans[n]
        span = pl.ds(start, size)
        wait(m.got.at[pl.ds(NC * lo, NC * (hi - lo)), :, pl.ds(2 * COLS, 2 * COLS)], m.r_up.at[n])
        total = m.half[span] + dot(
            m.got[NC * lo : NC * hi, :, 2 * COLS :].reshape(size, 2 * COLS),
            m.wgu[2 * COLS :],
        )
        pre = total[:, :HID]
        hidden = (pre / (1.0 + jnp.exp(-pre)) * total[:, HID:]).astype(BF16)
        m.hid[span] = hidden
        m.hids[span, 0:HID] = hidden
        for d in (2, 1, 3):
            send(
                m.hid.at[span],
                m.hids.at[span, pl.ds(HID * (NT - d), HID)],
                m.s_ag.at[n],
                m.r_ag.at[n],
                at(dt=d),
            )
    wait(m.dparts.at[pl.ds(1, NT - 1)], m.r_drs)
    pre = m.dpart[0, part(0)].astype(F32)
    up = m.dpart[1, part(0)].astype(F32)
    for d in range(1, NT):
        pre = pre + m.dparts[d, 0].astype(F32)
        up = up + m.dparts[d, 1].astype(F32)
    dhidden = (pre / (1.0 + jnp.exp(-pre)) * up).astype(BF16)
    m.dhid[...] = dhidden
    m.dhids[part(0)] = dhidden
    for d in (2, 1, 3):
        send(m.dhid, m.dhids.at[part(0)], m.s_dag, m.r_dag, at(dt=d))

    wait(m.wdn.at[pl.ds(1, NT - 1)], m.r_wdn)
    down = m.wdn[...].reshape(NT * HID, COLS)
    for n, (lo, hi) in enumerate(CHUNKS):
        start, size = spans[n]
        span = pl.ds(start, size)
        wait(m.hids.at[span, pl.ds(HID, (NT - 1) * HID)], m.r_ag.at[n])
        m.rows[NC * lo : NC * hi] = (
            dot(m.hids[span], down).astype(BF16).reshape(NC * (hi - lo), ROWS, COLS)
        )
        for spot in range(lo, hi):
            d = ORDER[spot]
            for e in range(NC):
                if d or e:
                    send(
                        m.rows.at[NC * spot + e],
                        m.back.at[NC * ((NZ - d) % NZ) + e],
                        m.s_rz,
                        m.r_rz,
                        at(a=d, dc=1) if e else at(b=d),
                    )
    m.back[0] = m.rows[NE - NC]

    gate = m.bgate[...].astype(F32)
    branch = jnp.zeros((ROWS, 128), F32)
    for j in range(WIDTH // 128):
        branch = branch + m.ffn[:, 128 * j : 128 * j + 128].astype(F32) * gate[j : j + 1]
    branch = jnp.sum(branch, axis=1, keepdims=True)
    branch = 1.0 / (1.0 + jnp.exp(-branch))
    wait(dense[2].at[pl.ds(1, NZ - 1)], m.r_dw.at[2])
    wait(m.dhids.at[pl.ds(0, 2 * gathered - quarter)], m.r_dag)
    m.dacc[...] = (
        dot(m.dhids[...], m.dd[...].reshape(NZ * DH, COLS))
        .astype(BF16)
        .reshape(NC * NY, ROWS, COLS)
    )
    for d in FAR + (0,):
        for e in range(NC):
            if d or e:
                send(
                    m.dacc.at[NY * e + d],
                    m.dfin.at[NY * e + (NY - d) % NY],
                    m.s_dy,
                    m.r_dy,
                    at(a=d, dc=e),
                )

    wait(m.back.at[pl.ds(1, NE - 1)], m.r_rz)
    both = dot_tn(m.weigh[...], m.back[...].reshape(NE * ROWS, COLS))
    m.acc[...] = both.astype(BF16).reshape(NY, ROWS, COLS)
    for d in FAR:
        send(m.acc.at[d], m.fin.at[NY - d], m.s_y, m.r_y, at(a=d))
    wait(m.dfin.at[pl.ds(1, NC * NY - 1)], m.r_dy)
    total = m.dacc[0].astype(F32)
    for d in range(1, NC * NY):
        total = total + m.dfin[d].astype(F32)
    total = m.after[:, block(0)] + branch * total + m.acc[0].astype(F32)
    wait(m.fin.at[pl.ds(1, NY - 1)], m.r_y)
    for d in range(1, NY):
        total = total + m.fin[d].astype(F32)
    out[...] = total.astype(BF16)

    wait(m.hp.at[pl.ds(1, NT - 1)], m.s_hp)
    wait(m.rt.at[pl.ds(1, NY - 1)], m.s_rt)
    wait(m.sc.at[pl.ds(1, NY - 1)], m.s_sc)
    wait(m.wdn.at[pl.ds(1, NT - 1)], m.s_wdn)
    wait(m.x.at[pl.ds(1, NY - 1)], m.s_x)
    wait(m.dx, m.s_dx)
    for k in range(3):
        wait(dense[k].at[pl.ds(1, NZ - 1)], m.s_dw.at[k])
    wait(m.got.at[pl.ds(1, NE - 1), :, left], m.s_z)
    for n, (lo, hi) in enumerate(CHUNKS):
        start, size = spans[n]
        span = pl.ds(start, size)
        wait(m.got.at[pl.ds(NC * lo, NC * (hi - lo)), :, pl.ds(2 * COLS, 2 * COLS)], m.s_up.at[n])
        wait(m.hids.at[span, pl.ds(HID, (NT - 1) * HID)], m.s_ag.at[n])
    wait(m.dparts.at[pl.ds(1, NT - 1)], m.s_drs)
    wait(m.dhids.at[pl.ds(0, 2 * gathered - quarter)], m.s_dag)
    wait(m.back.at[pl.ds(1, NE - 1)], m.s_rz)
    wait(m.dfin.at[pl.ds(1, NC * NY - 1)], m.s_dy)
    wait(m.fin.at[pl.ds(1, NY - 1)], m.s_y)


def on_device(
    tokens,
    positions,
    state,
    mix_gain,
    w_query,
    w_key,
    w_value,
    w_out,
    ffn_gain,
    branch_gate,
    dense_gate,
    dense_up,
    dense_down,
    routes,
    route_scores,
    expert_gate,
    expert_up,
    expert_down,
):
    half = HEAD // 2
    inverse = 10000.0 ** -(np.arange(half, dtype=np.float64) / (half - 1))
    freq = jnp.asarray(np.concatenate([inverse, inverse])[None], F32)
    args = (
        tokens,
        positions.reshape(1, ROWS),
        state.reshape(ROWS, HEAD, HEAD),
        mix_gain.reshape(WIDTH // 128, 128),
        w_query,
        w_key,
        w_value,
        w_out,
        ffn_gain.reshape(WIDTH // 128, 128),
        branch_gate.reshape(WIDTH // 128, 128),
        dense_gate.T,
        dense_up.T,
        dense_down,
        routes.T,
        route_scores.T,
        expert_gate.reshape(WIDTH, HID),
        expert_up.reshape(WIDTH, HID),
        expert_down.reshape(HID, WIDTH),
        freq,
    )
    return pl.pallas_call(
        kernel,
        name="layer",
        out_shape=pltpu.VMEM((ROWS, COLS), BF16),
        in_specs=[pl.BlockSpec(memory_space=pltpu.HBM)] * len(args),
        out_specs=pl.BlockSpec(memory_space=pltpu.VMEM),
        scratch_shapes=list(scratch_table().values()),
        compiler_params=pltpu.CompilerParams(
            collective_id=0, has_side_effects=True, vmem_limit_bytes=60 * 1024 * 1024
        ),
    )(*args)


def solution(mesh):
    placed = (
        P("ep", None),
        P("ep"),
        P("ep", "tp", None, None),
        P(),
        P(None, "tp"),
        P(None, "tp"),
        P(None, "tp"),
        P("tp", None),
        P(),
        P(),
        P("tp", "ep"),
        P("tp", "ep"),
        P("ep", "tp"),
        P("ep", None),
        P("ep", None),
        P("ep", None, "tp"),
        P("ep", None, "tp"),
        P("ep", "tp", None),
    )
    return jax.shard_map(
        on_device, mesh=mesh, in_specs=placed, out_specs=P("ep", "tp"), check_vma=False
    )
```

time: 65.1 us -> 59.6 us (0.916)
  Pallas kernels: 63.6 us -> 58.9 us
  local copies, waits for them, and re-layouts: 1.32 us -> 0.61 us
    pallas_call x1, Pallas kernels: 63.6 us -> 58.9 us  [on_device(): pl.pallas_call(kernel, name='layer', out_shape=pltpu.VMEM((ROWS, COLS), B...]
    unnamed x1, local copies, waits for them, and re-layouts: 1.32 us -> 0.61 us
where the time goes in v3:
time: 59.6 us; the launch traced here: 59.5 us
  Pallas kernels  58.9 us (99%)
  local copies, waits for them, and re-layouts  0.61 us (1%)
    pallas_call x1, Pallas kernels, on_device(): pl.pallas_call(kernel, name='layer', out_shape=pltpu.VMEM((ROWS, COLS), B...  58.9 us

profile of v3, /device:TPU:1, one launch (start us, length us, event | category | flops | bytes accessed | tf_op | source)
XLA Modules:
  0.0 59.5 jit_solution(1177418039558276336)
XLA Ops:
  0.0 58.9 %layer.1 = bf16[16,512]{1,0:T(8,128)(2,1)S(1)} custom-call(bf16[16,2048]{1,0:T(8,128)(2,1)} %tokens.1, s32[1,16]{1,0:T(1,128)} %bitcast.23, f32[16,128,128]{2,1,0:T(8,128)} %bitcast.12, f32[16,128]{1,0:T(8,128)} %bitcast.18, bf16[2048,128]{1,0:T(8,128)(2,1)} %w_query.1, bf16[2048,128]{1,0:T(8,128)(2,1)} %w_key.1, bf16[2048,128]{1,0:T(8,128)(2,1)} %w_value.1, ...), custom_call_target="tpu_custom_call" | custom-call | tf_op jit(solution)/shard_map/layer/pallas_call | solution.py:541
  58.9 0.6 %copy.21 = bf16[16,512]{1,0:T(8,128)(2,1)} copy(bf16[16,512]{1,0:T(8,128)(2,1)S(1)} %layer.1) | data formatting | bytes 32768

commit v4 on v3

--- a/solution.py
+++ b/solution.py
@@ -80,6 +80,8 @@
         dhids=pltpu.VMEM((2 * gathered, NZ * DH), BF16),
         dacc=pltpu.VMEM((NC * NY, ROWS, COLS), BF16),
         dfin=pltpu.VMEM((NC * NY, ROWS, COLS), BF16),
+        near=pltpu.SemaphoreType.REGULAR,
+        wide=pltpu.SemaphoreType.REGULAR,
         loc=dma((32,)),
         s_hp=dma,
         r_hp=dma,
@@ -190,15 +192,27 @@
     ]
 
     barrier = pltpu.get_barrier_semaphore()
-    peers = (
-        [at(dt=d) for d in range(1, NT)]
-        + [at(a=d) for d in range(1, NY)]
-        + [at(b=d) for d in range(1, NY)]
-        + [at(a=d, dc=1) for d in range(NY)]
-        + [at(b=d, dc=1) for d in range(1, NY)]
-    )
-    for dev in peers:
-        pl.semaphore_signal(barrier, 1, device_id=dev, device_id_type=MESH)
+
+    def greet(dz, dy, dx, core):
+        to = lax.rem(z + dz, NZ) * 16 + lax.rem(y + dy, NY) * 2 + core
+        pl.semaphore_signal(
+            barrier, 1, device_id=(to, lax.rem(t + dx, NT)), device_id_type=MESH
+        )
+
+    for d in range(1, NT):
+        greet(0, 0, d, 0)
+    for d in range(1, NY):
+        greet(0, d, 0, 1)
+    for d in range(1, NZ):
+        greet(d, 0, 0, 1)
+
+    @pl.when(c == 0)
+    def _():
+        greet(0, 0, 0, 1)
+
+    @pl.when(c == 1)
+    def _():
+        greet(0, 0, 0, 0)
 
     for copy in first:
         copy.wait()
@@ -247,107 +261,123 @@
     outs.wait()
     m.hp[0] = dot(retrieved.astype(BF16), m.wout[...]).astype(BF16)
 
-    pl.semaphore_wait(barrier, len(peers))
-
-    for d in (2, 1, 3):
-        send(m.hp.at[0], m.hp.at[NT - d], m.s_hp, m.r_hp, at(dt=d))
-    for d in range(1, NY):
-        send(routes, m.rt.at[NY - d], m.s_rt, m.r_rt, at(a=d))
-        send(scores, m.sc.at[NY - d], m.s_sc, m.r_sc, at(a=d))
+    gathered = NY * ROWS
+    quarter = 2 * gathered // NT
+    left = pl.ds(0, 2 * COLS)
+    right = pl.ds(2 * COLS, 2 * COLS)
     dense = (m.dg, m.du, m.dd)
 
-    def spread(k, src):
+    def part(d):
+        return pl.ds(pl.multiple_of(lax.rem(t + d, NT) * quarter, quarter), quarter)
+
+    def chunk_of(spot):
+        return [n for n, (lo, hi) in enumerate(CHUNKS) if lo <= spot < hi][0]
+
+    def spread(k):
+        src = (dense_gate, dense_up, dense_down)[k]
         for d in FAR:
             send(src, dense[k].at[NZ - d], m.s_dw.at[k], m.r_dw.at[k], at(b=d))
 
-    spread(0, dense_gate)
-
-    for copy in gains:
-        copy.wait()
-    wait(m.hp.at[pl.ds(1, NT - 1)], m.r_hp)
-    after = tok
-    for d in range(NT):
-        after = after + m.hp[d].astype(F32)
-    m.after[...] = after
-    scale = lax.rsqrt(jnp.mean(after * after, axis=1, keepdims=True) + EPS)
-    gain = m.ffng[...]
-    for j in range(WIDTH // 128):
-        m.ffn[:, 128 * j : 128 * j + 128] = (
-            after[:, 128 * j : 128 * j + 128] * scale * gain[j : j + 1]
-        ).astype(BF16)
-    for d in range(2):
-        m.x[0, :, COLS * d : COLS * (d + 1)] = m.ffn[:, block(d)]
-    for d in FAR:
-        send(m.x.at[0], m.x.at[NY - d], m.s_x, m.r_x, at(a=d))
-    for d in (2, 1, 3):
-        send(expert_down.at[:, block(d)], m.wdn.at[NT - d], m.s_wdn, m.r_wdn, at(dt=d))
-
-    for copy in own:
-        copy.wait()
-    wait(m.rt.at[pl.ds(1, NY - 1)], m.r_rt)
-    wait(m.sc.at[pl.ds(1, NY - 1)], m.r_sc)
-    chosen = jnp.concatenate([m.rt[d] for d in range(NY)], axis=1)
-    scored = jnp.concatenate([m.sc[d] for d in range(NY)], axis=1)
-    shares = scored / jnp.sum(scored, axis=0, keepdims=True)
-    k = lax.broadcasted_iota(jnp.int32, (NE, 128), 0)
-    lane = lax.broadcasted_iota(jnp.int32, (NE, 128), 1)
-    expert = (
-        ((z + (k // 2) * (1 - c)) & 7) * 16 + ((y + (k // 2) * c) & 7) * 2 + ((c + k) & 1)
-    )
-    named = jnp.zeros((NE, 128), F32)
-    share = jnp.zeros((NE, 128), F32)
-    for n in range(6):
-        hit = chosen[n : n + 1] == expert
-        named = jnp.where(hit, 1.0, named)
-        share = jnp.where(hit, shares[n : n + 1], share)
-    a = lax.broadcasted_iota(jnp.int32, (128, 128), 0)
-    b = lax.broadcasted_iota(jnp.int32, (128, 128), 1)
-    ahead = jnp.where((a // ROWS == b // ROWS) & (a < b), 1.0, 0.0).astype(BF16)
-    rank = dot(named.astype(BF16), ahead)
-    code = jnp.where(named > 0.5, rank + (2 * (lane // ROWS)).astype(F32), -1.0)
-    slot = lax.broadcasted_iota(jnp.int32, (ROWS, 128), 0).astype(F32)
-    for n in range(NE):
-        hit = code[n : n + 1] == slot
-        m.place[pl.ds(ROWS * n, ROWS), :] = jnp.where(hit, 1.0, 0.0).astype(BF16)
-        m.weigh[pl.ds(ROWS * n, ROWS), :] = jnp.where(hit, share[n : n + 1], 0.0).astype(BF16)
-
-    left = pl.ds(0, 2 * COLS)
-    wait(m.x.at[pl.ds(1, NY - 1)], m.r_x)
-    m.slots[...] = (
-        dot(m.place[...], m.x[...].reshape(NY * ROWS, 2 * COLS))
-        .astype(BF16)
-        .reshape(NE, ROWS, 2 * COLS)
-    )
-    m.got[NE - NC, :, left] = m.slots[0]
-
-    def chunk_of(spot):
-        return [n for n, (lo, hi) in enumerate(CHUNKS) if lo <= spot < hi][0]
-
-    for d in FAR + (0,):
-        spot = ORDER.index((NZ - d) % NZ)
-        for e in range(NC):
-            if d or e:
-                send(
-                    m.slots.at[NC * d + e],
-                    m.got.at[NC * spot + e, :, left],
-                    m.s_z,
-                    m.r_z.at[chunk_of(spot)],
-                    at(b=d, dc=e),
-                )
-    for d in FAR + (0,):
-        send(
-            m.x.at[0, :, pl.ds(0, COLS)], m.dx.at[(NY - d) % NY], m.s_dx, m.r_dx, at(b=d, dc=1)
-        )
-
-    spread(1, dense_up)
-
-    for copy in experts:
-        copy.wait()
-    spans = [(lo * NC * ROWS, (hi - lo) * NC * ROWS) for lo, hi in CHUNKS]
-    for n, (lo, hi) in enumerate(CHUNKS):
-        start, size = spans[n]
+    def spread_routes():
+        for d in FAR:
+            send(routes, m.rt.at[NY - d], m.s_rt, m.r_rt, at(a=d))
+            send(scores, m.sc.at[NY - d], m.s_sc, m.r_sc, at(a=d))
+
+    def split_down():
+        for d in (2, 1, 3):
+            send(expert_down.at[:, block(d)], m.wdn.at[NT - d], m.s_wdn, m.r_wdn, at(dt=d))
+
+    def mix():
+        for d in (2, 1, 3):
+            send(m.hp.at[0], m.hp.at[NT - d], m.s_hp, m.r_hp, at(dt=d))
+
+    def gather():
+        for copy in gains:
+            copy.wait()
+        wait(m.hp.at[pl.ds(1, NT - 1)], m.r_hp)
+        after = tok
+        for d in range(NT):
+            after = after + m.hp[d].astype(F32)
+        m.after[...] = after
+        scale = lax.rsqrt(jnp.mean(after * after, axis=1, keepdims=True) + EPS)
+        gain = m.ffng[...]
+        for j in range(WIDTH // 128):
+            m.ffn[:, 128 * j : 128 * j + 128] = (
+                after[:, 128 * j : 128 * j + 128] * scale * gain[j : j + 1]
+            ).astype(BF16)
+        for d in range(2):
+            m.x[0, :, COLS * d : COLS * (d + 1)] = m.ffn[:, block(d)]
+        for d in FAR:
+            send(m.x.at[0], m.x.at[NY - d], m.s_x, m.r_x, at(a=d))
+
+    def gather_other():
+        for d in FAR + (0,):
+            send(
+                m.x.at[0, :, pl.ds(0, COLS)],
+                m.dx.at[(NY - d) % NY],
+                m.s_dx,
+                m.r_dx,
+                at(b=d, dc=1),
+            )
+
+    def assign():
+        for copy in own:
+            copy.wait()
+        wait(m.rt.at[pl.ds(1, NY - 1)], m.r_rt)
+        wait(m.sc.at[pl.ds(1, NY - 1)], m.r_sc)
+        chosen = jnp.concatenate([m.rt[d] for d in range(NY)], axis=1)
+        scored = jnp.concatenate([m.sc[d] for d in range(NY)], axis=1)
+        shares = scored / jnp.sum(scored, axis=0, keepdims=True)
+        k = lax.broadcasted_iota(jnp.int32, (NE, 128), 0)
+        lane = lax.broadcasted_iota(jnp.int32, (NE, 128), 1)
+        expert = (
+            ((z + (k // 2) * (1 - c)) & 7) * 16 + ((y + (k // 2) * c) & 7) * 2 + ((c + k) & 1)
+        )
+        named = jnp.zeros((NE, 128), F32)
+        share = jnp.zeros((NE, 128), F32)
+        for n in range(6):
+            hit = chosen[n : n + 1] == expert
+            named = jnp.where(hit, 1.0, named)
+            share = jnp.where(hit, shares[n : n + 1], share)
+        a = lax.broadcasted_iota(jnp.int32, (128, 128), 0)
+        b = lax.broadcasted_iota(jnp.int32, (128, 128), 1)
+        ahead = jnp.where((a // ROWS == b // ROWS) & (a < b), 1.0, 0.0).astype(BF16)
+        rank = dot(named.astype(BF16), ahead)
+        code = jnp.where(named > 0.5, rank + (2 * (lane // ROWS)).astype(F32), -1.0)
+        slot = lax.broadcasted_iota(jnp.int32, (ROWS, 128), 0).astype(F32)
+        for n in range(NE):
+            hit = code[n : n + 1] == slot
+            m.place[pl.ds(ROWS * n, ROWS), :] = jnp.where(hit, 1.0, 0.0).astype(BF16)
+            m.weigh[pl.ds(ROWS * n, ROWS), :] = jnp.where(hit, share[n : n + 1], 0.0).astype(BF16)
+
+    def dispatch():
+        wait(m.x.at[pl.ds(1, NY - 1)], m.r_x)
+        m.slots[...] = (
+            dot(m.place[...], m.x[...].reshape(NY * ROWS, 2 * COLS))
+            .astype(BF16)
+            .reshape(NE, ROWS, 2 * COLS)
+        )
+        for spot, d in enumerate(ORDER):
+            for e in range(NC):
+                k = NC * ((NZ - d) % NZ) + e
+                if d or e:
+                    send(
+                        m.slots.at[k],
+                        m.got.at[NC * spot + e, :, left],
+                        m.s_z,
+                        m.r_z.at[chunk_of(spot)],
+                        at(b=(NZ - d) % NZ, dc=e),
+                    )
+                else:
+                    m.got[NC * spot, :, left] = m.slots[k]
+
+    def trade(n):
+        if n == 0:
+            for copy in experts:
+                copy.wait()
+        lo, hi = CHUNKS[n]
         some = pl.ds(NC * lo, NC * (hi - lo))
-        fresh = pl.ds(NC * lo, NC * (hi - lo) - (hi == NZ))
+        fresh = pl.ds(NC * lo, NC * (hi - lo) - (lo <= ORDER.index(0) < hi))
         wait(m.got.at[fresh, :, left], m.r_z.at[n])
         for k, d in ((0, 1), (1, 3)):
             send(
@@ -357,33 +387,17 @@
                 m.r_up.at[n],
                 at(dt=d),
             )
-        m.half[pl.ds(start, size)] = dot(
+        size = NC * ROWS * (hi - lo)
+        m.half[pl.ds(NC * ROWS * lo, size)] = dot(
             m.got[NC * lo : NC * hi, :, 0 : 2 * COLS].reshape(size, 2 * COLS),
             m.wgu[0 : 2 * COLS],
         )
-    spread(2, dense_down)
-
-    wait(m.dx, m.r_dx)
-    gathered = NY * ROWS
-    for k in range(2):
-        wait(dense[k].at[pl.ds(1, NZ - 1)], m.r_dw.at[k])
-        weights = dense[k][...].reshape(NZ * DH, COLS)
-        m.dpart[k, 0:gathered] = dot_nt(
-            m.x[:, :, 0:COLS].reshape(gathered, COLS), weights
-        ).astype(BF16)
-        m.dpart[k, gathered:] = dot_nt(m.dx[...].reshape(gathered, COLS), weights).astype(BF16)
-    quarter = 2 * gathered // NT
-
-    def part(d):
-        return pl.ds(pl.multiple_of(lax.rem(t + d, NT) * quarter, quarter), quarter)
-
-    for d in (2, 1, 3):
-        send(m.dpart.at[:, part(d)], m.dparts.at[NT - d], m.s_drs, m.r_drs, at(dt=d))
-
-    for n, (lo, hi) in enumerate(CHUNKS):
-        start, size = spans[n]
-        span = pl.ds(start, size)
-        wait(m.got.at[pl.ds(NC * lo, NC * (hi - lo)), :, pl.ds(2 * COLS, 2 * COLS)], m.r_up.at[n])
+
+    def hide(n):
+        lo, hi = CHUNKS[n]
+        size = NC * ROWS * (hi - lo)
+        span = pl.ds(NC * ROWS * lo, size)
+        wait(m.got.at[pl.ds(NC * lo, NC * (hi - lo)), :, right], m.r_up.at[n])
         total = m.half[span] + dot(
             m.got[NC * lo : NC * hi, :, 2 * COLS :].reshape(size, 2 * COLS),
             m.wgu[2 * COLS :],
@@ -400,26 +414,18 @@
                 m.r_ag.at[n],
                 at(dt=d),
             )
-    wait(m.dparts.at[pl.ds(1, NT - 1)], m.r_drs)
-    pre = m.dpart[0, part(0)].astype(F32)
-    up = m.dpart[1, part(0)].astype(F32)
-    for d in range(1, NT):
-        pre = pre + m.dparts[d, 0].astype(F32)
-        up = up + m.dparts[d, 1].astype(F32)
-    dhidden = (pre / (1.0 + jnp.exp(-pre)) * up).astype(BF16)
-    m.dhid[...] = dhidden
-    m.dhids[part(0)] = dhidden
-    for d in (2, 1, 3):
-        send(m.dhid, m.dhids.at[part(0)], m.s_dag, m.r_dag, at(dt=d))
-
-    wait(m.wdn.at[pl.ds(1, NT - 1)], m.r_wdn)
-    down = m.wdn[...].reshape(NT * HID, COLS)
-    for n, (lo, hi) in enumerate(CHUNKS):
-        start, size = spans[n]
-        span = pl.ds(start, size)
+
+    def answer(n):
+        if n == 0:
+            wait(m.wdn.at[pl.ds(1, NT - 1)], m.r_wdn)
+        lo, hi = CHUNKS[n]
+        size = NC * ROWS * (hi - lo)
+        span = pl.ds(NC * ROWS * lo, size)
         wait(m.hids.at[span, pl.ds(HID, (NT - 1) * HID)], m.r_ag.at[n])
         m.rows[NC * lo : NC * hi] = (
-            dot(m.hids[span], down).astype(BF16).reshape(NC * (hi - lo), ROWS, COLS)
+            dot(m.hids[span], m.wdn[...].reshape(NT * HID, COLS))
+            .astype(BF16)
+            .reshape(NC * (hi - lo), ROWS, COLS)
         )
         for spot in range(lo, hi):
             d = ORDER[spot]
@@ -432,46 +438,110 @@
                         m.r_rz,
                         at(a=d, dc=1) if e else at(b=d),
                     )
-    m.back[0] = m.rows[NE - NC]
-
-    gate = m.bgate[...].astype(F32)
-    branch = jnp.zeros((ROWS, 128), F32)
-    for j in range(WIDTH // 128):
-        branch = branch + m.ffn[:, 128 * j : 128 * j + 128].astype(F32) * gate[j : j + 1]
-    branch = jnp.sum(branch, axis=1, keepdims=True)
-    branch = 1.0 / (1.0 + jnp.exp(-branch))
-    wait(dense[2].at[pl.ds(1, NZ - 1)], m.r_dw.at[2])
-    wait(m.dhids.at[pl.ds(0, 2 * gathered - quarter)], m.r_dag)
-    m.dacc[...] = (
-        dot(m.dhids[...], m.dd[...].reshape(NZ * DH, COLS))
-        .astype(BF16)
-        .reshape(NC * NY, ROWS, COLS)
-    )
-    for d in FAR + (0,):
-        for e in range(NC):
-            if d or e:
-                send(
-                    m.dacc.at[NY * e + d],
-                    m.dfin.at[NY * e + (NY - d) % NY],
-                    m.s_dy,
-                    m.r_dy,
-                    at(a=d, dc=e),
-                )
-
-    wait(m.back.at[pl.ds(1, NE - 1)], m.r_rz)
-    both = dot_tn(m.weigh[...], m.back[...].reshape(NE * ROWS, COLS))
-    m.acc[...] = both.astype(BF16).reshape(NY, ROWS, COLS)
-    for d in FAR:
-        send(m.acc.at[d], m.fin.at[NY - d], m.s_y, m.r_y, at(a=d))
-    wait(m.dfin.at[pl.ds(1, NC * NY - 1)], m.r_dy)
-    total = m.dacc[0].astype(F32)
-    for d in range(1, NC * NY):
-        total = total + m.dfin[d].astype(F32)
-    total = m.after[:, block(0)] + branch * total + m.acc[0].astype(F32)
-    wait(m.fin.at[pl.ds(1, NY - 1)], m.r_y)
-    for d in range(1, NY):
-        total = total + m.fin[d].astype(F32)
-    out[...] = total.astype(BF16)
+                else:
+                    m.back[0] = m.rows[NC * spot]
+
+    def dense_in():
+        wait(m.dx, m.r_dx)
+        for k in range(2):
+            wait(dense[k].at[pl.ds(1, NZ - 1)], m.r_dw.at[k])
+            weights = dense[k][...].reshape(NZ * DH, COLS)
+            m.dpart[k, 0:gathered] = dot_nt(
+                m.x[:, :, 0:COLS].reshape(gathered, COLS), weights
+            ).astype(BF16)
+            m.dpart[k, gathered:] = dot_nt(m.dx[...].reshape(gathered, COLS), weights).astype(BF16)
+        for d in (2, 1, 3):
+            send(m.dpart.at[:, part(d)], m.dparts.at[NT - d], m.s_drs, m.r_drs, at(dt=d))
+
+    def dense_hide():
+        wait(m.dparts.at[pl.ds(1, NT - 1)], m.r_drs)
+        pre = m.dpart[0, part(0)].astype(F32)
+        up = m.dpart[1, part(0)].astype(F32)
+        for d in range(1, NT):
+            pre = pre + m.dparts[d, 0].astype(F32)
+            up = up + m.dparts[d, 1].astype(F32)
+        dhidden = (pre / (1.0 + jnp.exp(-pre)) * up).astype(BF16)
+        m.dhid[...] = dhidden
+        m.dhids[part(0)] = dhidden
+        for d in (2, 1, 3):
+            send(m.dhid, m.dhids.at[part(0)], m.s_dag, m.r_dag, at(dt=d))
+
+    def dense_out():
+        wait(dense[2].at[pl.ds(1, NZ - 1)], m.r_dw.at[2])
+        wait(m.dhids.at[pl.ds(0, 2 * gathered - quarter)], m.r_dag)
+        m.dacc[...] = (
+            dot(m.dhids[...], m.dd[...].reshape(NZ * DH, COLS))
+            .astype(BF16)
+            .reshape(NC * NY, ROWS, COLS)
+        )
+        for d in FAR + (0,):
+            for e in range(NC):
+                if d or e:
+                    send(
+                        m.dacc.at[NY * e + d],
+                        m.dfin.at[NY * e + (NY - d) % NY],
+                        m.s_dy,
+                        m.r_dy,
+                        at(a=d, dc=e),
+                    )
+
+    def finish():
+        wait(m.back.at[pl.ds(1, NE - 1)], m.r_rz)
+        both = dot_tn(m.weigh[...], m.back[...].reshape(NE * ROWS, COLS))
+        m.acc[...] = both.astype(BF16).reshape(NY, ROWS, COLS)
+        for d in FAR:
+            send(m.acc.at[d], m.fin.at[NY - d], m.s_y, m.r_y, at(a=d))
+        gate = m.bgate[...].astype(F32)
+        branch = jnp.zeros((ROWS, 128), F32)
+        for j in range(WIDTH // 128):
+            branch = branch + m.ffn[:, 128 * j : 128 * j + 128].astype(F32) * gate[j : j + 1]
+        branch = jnp.sum(branch, axis=1, keepdims=True)
+        branch = 1.0 / (1.0 + jnp.exp(-branch))
+        wait(m.dfin.at[pl.ds(1, NC * NY - 1)], m.r_dy)
+        total = m.dacc[0].astype(F32)
+        for d in range(1, NC * NY):
+            total = total + m.dfin[d].astype(F32)
+        total = m.after[:, block(0)] + branch * total + m.acc[0].astype(F32)
+        wait(m.fin.at[pl.ds(1, NY - 1)], m.r_y)
+        for d in range(1, NY):
+            total = total + m.fin[d].astype(F32)
+        out[...] = total.astype(BF16)
+
+    def meet(core, count, sem):
+        @pl.when(c == core)
+        def _():
+            pl.semaphore_wait(barrier, count)
+            pl.semaphore_signal(sem, 1, device_id=at(dc=1), device_id_type=MESH)
+
+        @pl.when(c != core)
+        def _():
+            pl.semaphore_wait(sem, 1)
+
+    meet(0, NC * (NT - 1) + 1, m.near)
+    mix()
+    meet(1, NC * (NY - 1 + NZ - 1) + 1, m.wide)
+    spread_routes()
+    spread(0)
+    gather()
+    split_down()
+    assign()
+    dispatch()
+    gather_other()
+    spread(1)
+    trade(0)
+    trade(1)
+    trade(2)
+    spread(2)
+    dense_in()
+    hide(0)
+    hide(1)
+    hide(2)
+    dense_hide()
+    answer(0)
+    answer(1)
+    answer(2)
+    dense_out()
+    finish()
 
     wait(m.hp.at[pl.ds(1, NT - 1)], m.s_hp)
     wait(m.rt.at[pl.ds(1, NY - 1)], m.s_rt)
@@ -483,9 +553,8 @@
         wait(dense[k].at[pl.ds(1, NZ - 1)], m.s_dw.at[k])
     wait(m.got.at[pl.ds(1, NE - 1), :, left], m.s_z)
     for n, (lo, hi) in enumerate(CHUNKS):
-        start, size = spans[n]
-        span = pl.ds(start, size)
-        wait(m.got.at[pl.ds(NC * lo, NC * (hi - lo)), :, pl.ds(2 * COLS, 2 * COLS)], m.s_up.at[n])
+        span = pl.ds(NC * ROWS * lo, NC * ROWS * (hi - lo))
+        wait(m.got.at[pl.ds(NC * lo, NC * (hi - lo)), :, right], m.s_up.at[n])
         wait(m.hids.at[span, pl.ds(HID, (NT - 1) * HID)], m.s_ag.at[n])
     wait(m.dparts.at[pl.ds(1, NT - 1)], m.s_drs)
     wait(m.dhids.at[pl.ds(0, 2 * gathered - quarter)], m.s_dag)

time: 59.6 us -> 58.6 us (0.983)
  Pallas kernels: 58.9 us -> 57.6 us
    pallas_call x1, Pallas kernels: 58.9 us -> 57.6 us  [on_device(): pl.pallas_call(kernel, name='layer', out_shape=pltpu.VMEM((ROWS, COLS), B...]
where the time goes in v4:
time: 58.6 us; the launch traced here: 58.2 us
  Pallas kernels  57.6 us (98%)
  local copies, waits for them, and re-layouts  0.61 us (1%)
    pallas_call x1, Pallas kernels, on_device(): pl.pallas_call(kernel, name='layer', out_shape=pltpu.VMEM((ROWS, COLS), B...  57.6 us

profile of v4, /device:TPU:1, one launch (start us, length us, event | category | flops | bytes accessed | tf_op | source)
XLA Modules:
  0.0 58.2 jit_solution(10084994314107034034)
XLA Ops:
  0.0 57.6 %layer.1 = bf16[16,512]{1,0:T(8,128)(2,1)S(1)} custom-call(bf16[16,2048]{1,0:T(8,128)(2,1)} %tokens.1, s32[1,16]{1,0:T(1,128)} %bitcast.23, f32[16,128,128]{2,1,0:T(8,128)} %bitcast.12, f32[16,128]{1,0:T(8,128)} %bitcast.18, bf16[2048,128]{1,0:T(8,128)(2,1)} %w_query.1, bf16[2048,128]{1,0:T(8,128)(2,1)} %w_key.1, bf16[2048,128]{1,0:T(8,128)(2,1)} %w_value.1, ...), custom_call_target="tpu_custom_call" | custom-call | tf_op jit(solution)/shard_map/layer/pallas_call | solution.py:610
  57.6 0.6 %copy.21 = bf16[16,512]{1,0:T(8,128)(2,1)} copy(bf16[16,512]{1,0:T(8,128)(2,1)S(1)} %layer.1) | data formatting | bytes 32768

commit v5 on v4

--- a/solution.py
+++ b/solution.py
@@ -20,8 +20,8 @@
 HID = 128
 DH = 32
 NE = NZ * NC
-ORDER = (4, 3, 5, 2, 6, 1, 7, 0)
-CHUNKS = ((0, 3), (3, 5), (5, 8))
+ORDER = (0, 1, 7, 2, 6, 3, 5, 4)
+CHUNKS = ((0, 3), (3, 5), (5, 7), (7, 8))
 FAR = (4, 3, 5, 2, 6, 1, 7)
 
 def dot(a, b):
@@ -82,7 +82,7 @@
         dfin=pltpu.VMEM((NC * NY, ROWS, COLS), BF16),
         near=pltpu.SemaphoreType.REGULAR,
         wide=pltpu.SemaphoreType.REGULAR,
-        loc=dma((32,)),
+        loc=dma((16,)),
         s_hp=dma,
         r_hp=dma,
         s_wdn=dma,
@@ -99,9 +99,9 @@
         r_dw=dma((3,)),
         s_z=dma,
         r_z=dma((nch,)),
-        s_up=dma((nch,)),
+        s_up=dma,
         r_up=dma((nch,)),
-        s_ag=dma((nch,)),
+        s_ag=dma,
         r_ag=dma((nch,)),
         s_rz=dma,
         r_rz=dma,
@@ -160,36 +160,23 @@
     def block(d):
         return pl.ds(pl.multiple_of(lax.rem(t + d, NT) * COLS, COLS), COLS)
 
-    count = [0]
-
-    def fetch(src, dst):
-        copy = pltpu.make_async_copy(src, dst, m.loc.at[count[0]])
-        count[0] += 1
-        copy.start()
-        return copy
-
-    first = [fetch(tokens, m.tok), fetch(mix_gain, m.mixg)]
-    qkv = [
-        fetch(n, m.wqkv.at[:, pl.ds(HEAD * k, HEAD)])
-        for k, n in enumerate((w_query, w_key, w_value))
-    ]
-    turn = [fetch(positions, m.pos), fetch(freq, m.freq)]
-    states = fetch(state, m.state)
-    outs = fetch(w_out, m.wout)
-    gains = [fetch(ffn_gain, m.ffng), fetch(branch_gate, m.bgate)]
-    own = [
-        fetch(routes, m.rt.at[0]),
-        fetch(scores, m.sc.at[0]),
-        fetch(expert_down.at[:, block(0)], m.wdn.at[0]),
-        fetch(dense_gate, m.dg.at[0]),
-        fetch(dense_up, m.du.at[0]),
-        fetch(dense_down, m.dd.at[0]),
-    ]
-    experts = [
-        fetch(n.at[block(d)], m.wgu.at[pl.ds(COLS * d, COLS), pl.ds(HID * k, HID)])
-        for d in range(NT)
-        for k, n in enumerate((expert_gate, expert_up))
-    ]
+    def fetch(k, *pairs):
+        for src, dst in pairs:
+            pltpu.make_async_copy(src, dst, m.loc.at[k]).start()
+
+    fetch(0, (tokens, m.tok))
+    fetch(1, (mix_gain, m.mixg))
+    fetch(2, (positions, m.pos))
+    fetch(3, (freq, m.freq))
+    fetch(
+        4,
+        *[
+            (n, m.wqkv.at[:, pl.ds(HEAD * k, HEAD)])
+            for k, n in enumerate((w_query, w_key, w_value))
+        ],
+    )
+    fetch(5, (state, m.state))
+    fetch(6, (w_out, m.wout))
 
     barrier = pltpu.get_barrier_semaphore()
 
@@ -214,8 +201,8 @@
     def _():
         greet(0, 0, 0, 0)
 
-    for copy in first:
-        copy.wait()
+    wait(m.tok, m.loc.at[0])
+    wait(m.mixg, m.loc.at[1])
     tok = m.tok[...].astype(F32)
     scale = lax.rsqrt(jnp.mean(tok * tok, axis=1, keepdims=True) + EPS)
     gain = m.mixg[...]
@@ -226,8 +213,8 @@
         ],
         axis=1,
     )
-    for copy in turn:
-        copy.wait()
+    wait(m.pos, m.loc.at[2])
+    wait(m.freq, m.loc.at[3])
     eye = lax.broadcasted_iota(jnp.int32, (ROWS, ROWS), 0) == lax.broadcasted_iota(
         jnp.int32, (ROWS, ROWS), 1
     )
@@ -236,8 +223,7 @@
     lane = lax.broadcasted_iota(jnp.int32, (ROWS, HEAD), 1)
     cosine = jnp.cos(angle)
     sine = jnp.where(lane < HEAD // 2, -jnp.sin(angle), jnp.sin(angle))
-    for copy in qkv:
-        copy.wait()
+    wait(m.wqkv, m.loc.at[4])
     qkv = dot(normed, m.wqkv[...])
     query, key, value = (qkv[:, HEAD * k : HEAD * (k + 1)] for k in range(3))
 
@@ -249,7 +235,7 @@
     head = t.astype(F32)
     decay = 1.0 - jnp.exp2(jnp.full((1, HEAD), -5.0 - 5.0 * head / (NT - 1), F32))
     columns = query.T
-    states.wait()
+    wait(m.state, m.loc.at[5])
     for s in range(ROWS):
         m.ret[pl.ds(s, 1), :] = jnp.sum(
             m.state[s] * columns[:, s : s + 1], axis=0, keepdims=True
@@ -258,7 +244,22 @@
     retrieved = retrieved * lax.rsqrt(
         jnp.mean(retrieved * retrieved, axis=1, keepdims=True) + EPS
     )
-    outs.wait()
+    fetch(7, (ffn_gain, m.ffng))
+    fetch(8, (routes, m.rt.at[0]))
+    fetch(9, (scores, m.sc.at[0]))
+    fetch(10, (expert_down.at[:, block(0)], m.wdn.at[0]))
+    for k, (src, dst) in enumerate(((dense_gate, m.dg), (dense_up, m.du), (dense_down, m.dd))):
+        fetch(11 + k, (src, dst.at[0]))
+    fetch(14, (branch_gate, m.bgate))
+    fetch(
+        15,
+        *[
+            (n.at[block(d)], m.wgu.at[pl.ds(COLS * d, COLS), pl.ds(HID * k, HID)])
+            for d in range(NT)
+            for k, n in enumerate((expert_gate, expert_up))
+        ],
+    )
+    wait(m.wout, m.loc.at[6])
     m.hp[0] = dot(retrieved.astype(BF16), m.wout[...]).astype(BF16)
 
     gathered = NY * ROWS
@@ -292,8 +293,7 @@
             send(m.hp.at[0], m.hp.at[NT - d], m.s_hp, m.r_hp, at(dt=d))
 
     def gather():
-        for copy in gains:
-            copy.wait()
+        wait(m.ffng, m.loc.at[7])
         wait(m.hp.at[pl.ds(1, NT - 1)], m.r_hp)
         after = tok
         for d in range(NT):
@@ -321,8 +321,8 @@
             )
 
     def assign():
-        for copy in own:
-            copy.wait()
+        wait(m.rt.at[0], m.loc.at[8])
+        wait(m.sc.at[0], m.loc.at[9])
         wait(m.rt.at[pl.ds(1, NY - 1)], m.r_rt)
         wait(m.sc.at[pl.ds(1, NY - 1)], m.r_sc)
         chosen = jnp.concatenate([m.rt[d] for d in range(NY)], axis=1)
@@ -373,8 +373,7 @@
 
     def trade(n):
         if n == 0:
-            for copy in experts:
-                copy.wait()
+            wait(m.wgu, m.loc.at[15])
         lo, hi = CHUNKS[n]
         some = pl.ds(NC * lo, NC * (hi - lo))
         fresh = pl.ds(NC * lo, NC * (hi - lo) - (lo <= ORDER.index(0) < hi))
@@ -383,7 +382,7 @@
             send(
                 m.got.at[some, :, pl.ds(COLS * k, COLS)],
                 m.got.at[some, :, pl.ds(COLS * (3 - k), COLS)],
-                m.s_up.at[n],
+                m.s_up,
                 m.r_up.at[n],
                 at(dt=d),
             )
@@ -410,13 +409,14 @@
             send(
                 m.hid.at[span],
                 m.hids.at[span, pl.ds(HID * (NT - d), HID)],
-                m.s_ag.at[n],
+                m.s_ag,
                 m.r_ag.at[n],
                 at(dt=d),
             )
 
     def answer(n):
         if n == 0:
+            wait(m.wdn.at[0], m.loc.at[10])
             wait(m.wdn.at[pl.ds(1, NT - 1)], m.r_wdn)
         lo, hi = CHUNKS[n]
         size = NC * ROWS * (hi - lo)
@@ -444,6 +444,7 @@
     def dense_in():
         wait(m.dx, m.r_dx)
         for k in range(2):
+            wait(dense[k].at[0], m.loc.at[11 + k])
             wait(dense[k].at[pl.ds(1, NZ - 1)], m.r_dw.at[k])
             weights = dense[k][...].reshape(NZ * DH, COLS)
             m.dpart[k, 0:gathered] = dot_nt(
@@ -467,6 +468,7 @@
             send(m.dhid, m.dhids.at[part(0)], m.s_dag, m.r_dag, at(dt=d))
 
     def dense_out():
+        wait(dense[2].at[0], m.loc.at[13])
         wait(dense[2].at[pl.ds(1, NZ - 1)], m.r_dw.at[2])
         wait(m.dhids.at[pl.ds(0, 2 * gathered - quarter)], m.r_dag)
         m.dacc[...] = (
@@ -491,6 +493,7 @@
         m.acc[...] = both.astype(BF16).reshape(NY, ROWS, COLS)
         for d in FAR:
             send(m.acc.at[d], m.fin.at[NY - d], m.s_y, m.r_y, at(a=d))
+        wait(m.bgate, m.loc.at[14])
         gate = m.bgate[...].astype(F32)
         branch = jnp.zeros((ROWS, 128), F32)
         for j in range(WIDTH // 128):
@@ -522,24 +525,27 @@
     meet(1, NC * (NY - 1 + NZ - 1) + 1, m.wide)
     spread_routes()
     spread(0)
+    spread(1)
     gather()
+    gather_other()
     split_down()
     assign()
     dispatch()
-    gather_other()
-    spread(1)
+    dense_in()
     trade(0)
     trade(1)
     trade(2)
+    trade(3)
     spread(2)
-    dense_in()
     hide(0)
     hide(1)
     hide(2)
+    hide(3)
     dense_hide()
     answer(0)
     answer(1)
     answer(2)
+    answer(3)
     dense_out()
     finish()
 
@@ -552,10 +558,8 @@
     for k in range(3):
         wait(dense[k].at[pl.ds(1, NZ - 1)], m.s_dw.at[k])
     wait(m.got.at[pl.ds(1, NE - 1), :, left], m.s_z)
-    for n, (lo, hi) in enumerate(CHUNKS):
-        span = pl.ds(NC * ROWS * lo, NC * ROWS * (hi - lo))
-        wait(m.got.at[pl.ds(NC * lo, NC * (hi - lo)), :, right], m.s_up.at[n])
-        wait(m.hids.at[span, pl.ds(HID, (NT - 1) * HID)], m.s_ag.at[n])
+    wait(m.got.at[:, :, right], m.s_up)
+    wait(m.hids.at[:, pl.ds(HID, (NT - 1) * HID)], m.s_ag)
     wait(m.dparts.at[pl.ds(1, NT - 1)], m.s_drs)
     wait(m.dhids.at[pl.ds(0, 2 * gathered - quarter)], m.s_dag)
     wait(m.back.at[pl.ds(1, NE - 1)], m.s_rz)

time: 58.6 us -> 56.1 us (0.957)
  Pallas kernels: 57.6 us -> 55.4 us
    pallas_call x1, Pallas kernels: 57.6 us -> 55.4 us  [on_device(): pl.pallas_call(kernel, name='layer', out_shape=pltpu.VMEM((ROWS, COLS), B...]
where the time goes in v5:
time: 56.1 us; the launch traced here: 56 us
  Pallas kernels  55.4 us (99%)
  local copies, waits for them, and re-layouts  0.61 us (1%)
    pallas_call x1, Pallas kernels, on_device(): pl.pallas_call(kernel, name='layer', out_shape=pltpu.VMEM((ROWS, COLS), B...  55.4 us

profile of v5, /device:TPU:1, one launch (start us, length us, event | category | flops | bytes accessed | tf_op | source)
XLA Modules:
  0.0 56.0 jit_solution(4849391969883842512)
XLA Ops:
  0.0 55.4 %layer.1 = bf16[16,512]{1,0:T(8,128)(2,1)S(1)} custom-call(bf16[16,2048]{1,0:T(8,128)(2,1)} %tokens.1, s32[1,16]{1,0:T(1,128)} %bitcast.23, f32[16,128,128]{2,1,0:T(8,128)} %bitcast.12, f32[16,128]{1,0:T(8,128)} %bitcast.18, bf16[2048,128]{1,0:T(8,128)(2,1)} %w_query.1, bf16[2048,128]{1,0:T(8,128)(2,1)} %w_key.1, bf16[2048,128]{1,0:T(8,128)(2,1)} %w_value.1, ...), custom_call_target="tpu_custom_call" | custom-call | tf_op jit(solution)/shard_map/layer/pallas_call | solution.py:614
  55.4 0.6 %copy.21 = bf16[16,512]{1,0:T(8,128)(2,1)} copy(bf16[16,512]{1,0:T(8,128)(2,1)S(1)} %layer.1) | data formatting | bytes 32768

commit v6 on v5

--- a/solution.py
+++ b/solution.py
@@ -20,9 +20,11 @@
 HID = 128
 DH = 32
 NE = NZ * NC
-ORDER = (0, 1, 7, 2, 6, 3, 5, 4)
-CHUNKS = ((0, 3), (3, 5), (5, 7), (7, 8))
+HALF = NZ // 2
+WAVES = 2
+UNIT = 8
 FAR = (4, 3, 5, 2, 6, 1, 7)
+
 
 def dot(a, b):
     return jnp.dot(a, b, preferred_element_type=F32)
@@ -38,8 +40,8 @@
 
 def scratch_table():
     dma = pltpu.SemaphoreType.DMA
-    nch = len(CHUNKS)
     gathered = NY * ROWS
+    wave = NE * UNIT
     return dict(
         tok=pltpu.VMEM((ROWS, WIDTH), BF16),
         pos=pltpu.VMEM((1, ROWS), jnp.int32),
@@ -50,24 +52,23 @@
         ffng=pltpu.VMEM((WIDTH // 128, 128), F32),
         bgate=pltpu.VMEM((WIDTH // 128, 128), BF16),
         freq=pltpu.VMEM((1, 128), F32),
-        ret=pltpu.VMEM((ROWS, HEAD), F32),
         hp=pltpu.VMEM((NT, ROWS, WIDTH), BF16),
         after=pltpu.VMEM((ROWS, WIDTH), F32),
         ffn=pltpu.VMEM((ROWS, WIDTH), BF16),
         x=pltpu.VMEM((NY, ROWS, 2 * COLS), BF16),
         rt=pltpu.VMEM((NY, 6, ROWS), jnp.int32),
         sc=pltpu.VMEM((NY, 6, ROWS), F32),
-        place=pltpu.VMEM((NE * ROWS, 128), BF16),
-        weigh=pltpu.VMEM((NE * ROWS, 128), BF16),
-        slots=pltpu.VMEM((NE, ROWS, 2 * COLS), BF16),
-        got=pltpu.VMEM((NE, ROWS, WIDTH), BF16),
+        place=pltpu.VMEM((2, wave, gathered // 2), BF16),
+        weigh=pltpu.VMEM((2, wave, gathered // 2), BF16),
+        slots=pltpu.VMEM((2, NE, UNIT, 2 * COLS), BF16),
+        got=pltpu.VMEM((WAVES, NE, UNIT, WIDTH), BF16),
         wgu=pltpu.VMEM((WIDTH, 2 * HID), BF16),
         wdn=pltpu.VMEM((NT, HID, COLS), BF16),
-        half=pltpu.VMEM((NE * ROWS, 2 * HID), F32),
-        hid=pltpu.VMEM((NE * ROWS, HID), BF16),
-        hids=pltpu.VMEM((NE * ROWS, NT * HID), BF16),
-        rows=pltpu.VMEM((NE, ROWS, COLS), BF16),
-        back=pltpu.VMEM((NE, ROWS, COLS), BF16),
+        half=pltpu.VMEM((WAVES, wave, 2 * HID), F32),
+        hid=pltpu.VMEM((WAVES, wave, HID), BF16),
+        hids=pltpu.VMEM((WAVES, wave, NT * HID), BF16),
+        rows=pltpu.VMEM((WAVES, NE, UNIT, COLS), BF16),
+        back=pltpu.VMEM((2, NE, UNIT, COLS), BF16),
         acc=pltpu.VMEM((NY, ROWS, COLS), BF16),
         fin=pltpu.VMEM((NY, ROWS, COLS), BF16),
         dx=pltpu.VMEM((NY, ROWS, COLS), BF16),
@@ -92,19 +93,19 @@
         s_sc=dma,
         r_sc=dma,
         s_x=dma,
-        r_x=dma,
+        r_x=dma((2,)),
         s_dx=dma,
         r_dx=dma,
         s_dw=dma((3,)),
         r_dw=dma((3,)),
         s_z=dma,
-        r_z=dma((nch,)),
+        r_z=dma((2 * WAVES,)),
         s_up=dma,
-        r_up=dma((nch,)),
+        r_up=dma((2 * WAVES,)),
         s_ag=dma,
-        r_ag=dma((nch,)),
+        r_ag=dma((2 * WAVES,)),
         s_rz=dma,
-        r_rz=dma,
+        r_rz=dma((2,)),
         s_drs=dma,
         r_drs=dma,
         s_dag=dma,
@@ -160,6 +161,10 @@
     def block(d):
         return pl.ds(pl.multiple_of(lax.rem(t + d, NT) * COLS, COLS), COLS)
 
+    near_half = z // HALF
+    mine_a = y * (1 - c) + z * c
+    mine_b = z * (1 - c) + y * c
+
     def fetch(k, *pairs):
         for src, dst in pairs:
             pltpu.make_async_copy(src, dst, m.loc.at[k]).start()
@@ -234,19 +239,19 @@
     key = rotate(key) * HEAD**-0.5
     head = t.astype(F32)
     decay = 1.0 - jnp.exp2(jnp.full((1, HEAD), -5.0 - 5.0 * head / (NT - 1), F32))
-    columns = query.T
+    row = lax.broadcasted_iota(jnp.int32, (ROWS, HEAD), 0)
+    apart = jnp.concatenate(
+        [jnp.where(row == s, query, 0.0).astype(BF16) for s in range(ROWS)], axis=1
+    )
     wait(m.state, m.loc.at[5])
-    for s in range(ROWS):
-        m.ret[pl.ds(s, 1), :] = jnp.sum(
-            m.state[s] * columns[:, s : s + 1], axis=0, keepdims=True
-        )
-    retrieved = m.ret[...] * decay + jnp.sum(query * key, axis=1, keepdims=True) * value
+    held = dot(apart, m.state[...].reshape(ROWS * HEAD, HEAD).astype(BF16))
+    retrieved = held * decay + jnp.sum(query * key, axis=1, keepdims=True) * value
     retrieved = retrieved * lax.rsqrt(
         jnp.mean(retrieved * retrieved, axis=1, keepdims=True) + EPS
     )
     fetch(7, (ffn_gain, m.ffng))
-    fetch(8, (routes, m.rt.at[0]))
-    fetch(9, (scores, m.sc.at[0]))
+    fetch(8, (routes, m.rt.at[mine_a]))
+    fetch(9, (scores, m.sc.at[mine_a]))
     fetch(10, (expert_down.at[:, block(0)], m.wdn.at[0]))
     for k, (src, dst) in enumerate(((dense_gate, m.dg), (dense_up, m.du), (dense_down, m.dd))):
         fetch(11 + k, (src, dst.at[0]))
@@ -271,9 +276,6 @@
     def part(d):
         return pl.ds(pl.multiple_of(lax.rem(t + d, NT) * quarter, quarter), quarter)
 
-    def chunk_of(spot):
-        return [n for n, (lo, hi) in enumerate(CHUNKS) if lo <= spot < hi][0]
-
     def spread(k):
         src = (dense_gate, dense_up, dense_down)[k]
         for d in FAR:
@@ -281,8 +283,8 @@
 
     def spread_routes():
         for d in FAR:
-            send(routes, m.rt.at[NY - d], m.s_rt, m.r_rt, at(a=d))
-            send(scores, m.sc.at[NY - d], m.s_sc, m.r_sc, at(a=d))
+            send(routes, m.rt.at[mine_a], m.s_rt, m.r_rt, at(a=d))
+            send(scores, m.sc.at[mine_a], m.s_sc, m.r_sc, at(a=d))
 
     def split_down():
         for d in (2, 1, 3):
@@ -306,15 +308,15 @@
                 after[:, 128 * j : 128 * j + 128] * scale * gain[j : j + 1]
             ).astype(BF16)
         for d in range(2):
-            m.x[0, :, COLS * d : COLS * (d + 1)] = m.ffn[:, block(d)]
+            m.x[mine_a, :, COLS * d : COLS * (d + 1)] = m.ffn[:, block(d)]
         for d in FAR:
-            send(m.x.at[0], m.x.at[NY - d], m.s_x, m.r_x, at(a=d))
+            send(m.x.at[mine_a], m.x.at[mine_a], m.s_x, m.r_x.at[mine_a // HALF], at(a=d))
 
     def gather_other():
         for d in FAR + (0,):
             send(
-                m.x.at[0, :, pl.ds(0, COLS)],
-                m.dx.at[(NY - d) % NY],
+                m.x.at[mine_a, :, pl.ds(0, COLS)],
+                m.dx.at[mine_b],
                 m.s_dx,
                 m.r_dx,
                 at(b=d, dc=1),
@@ -325,121 +327,190 @@
         wait(m.sc.at[0], m.loc.at[9])
         wait(m.rt.at[pl.ds(1, NY - 1)], m.r_rt)
         wait(m.sc.at[pl.ds(1, NY - 1)], m.r_sc)
-        chosen = jnp.concatenate([m.rt[d] for d in range(NY)], axis=1)
-        scored = jnp.concatenate([m.sc[d] for d in range(NY)], axis=1)
-        shares = scored / jnp.sum(scored, axis=0, keepdims=True)
-        k = lax.broadcasted_iota(jnp.int32, (NE, 128), 0)
-        lane = lax.broadcasted_iota(jnp.int32, (NE, 128), 1)
-        expert = (
-            ((z + (k // 2) * (1 - c)) & 7) * 16 + ((y + (k // 2) * c) & 7) * 2 + ((c + k) & 1)
+        tokens_h = HALF * ROWS
+        k = lax.broadcasted_iota(jnp.int32, (NE, tokens_h), 0)
+        lane = lax.broadcasted_iota(jnp.int32, (NE, tokens_h), 1)
+        expert = ((k // 2) * (1 - c) + z * c) * 16 + ((k // 2) * c + y * (1 - c)) * 2 + (k & 1)
+        a = lax.broadcasted_iota(jnp.int32, (tokens_h, tokens_h), 0)
+        b = lax.broadcasted_iota(jnp.int32, (tokens_h, tokens_h), 1)
+        ahead = jnp.where((a // ROWS == b // ROWS) & (a < b), 1.0, 0.0).astype(BF16)
+        slot = lax.broadcasted_iota(jnp.int32, (UNIT, tokens_h), 0).astype(F32)
+        for h in range(2):
+            some = range(HALF * h, HALF * (h + 1))
+            chosen = jnp.concatenate([m.rt[d] for d in some], axis=1)
+            scored = jnp.concatenate([m.sc[d] for d in some], axis=1)
+            shares = scored / jnp.sum(scored, axis=0, keepdims=True)
+            named = jnp.zeros((NE, tokens_h), F32)
+            share = jnp.zeros((NE, tokens_h), F32)
+            for n in range(6):
+                hit = chosen[n : n + 1] == expert
+                named = jnp.where(hit, 1.0, named)
+                share = jnp.where(hit, shares[n : n + 1], share)
+            rank = dot(named.astype(BF16), ahead)
+            code = jnp.where(named > 0.5, rank + (2 * (lane // ROWS)).astype(F32), -1.0)
+            for n in range(NE):
+                hit = code[n : n + 1] == slot
+                at_n = pl.ds(UNIT * n, UNIT)
+                m.place[h, at_n, :] = jnp.where(hit, 1.0, 0.0).astype(BF16)
+                m.weigh[h, at_n, :] = jnp.where(hit, share[n : n + 1], 0.0).astype(BF16)
+
+    def emit(h):
+        inside = mine_a // HALF == h
+
+        @pl.when(inside)
+        def _():
+            wait(m.x.at[pl.ds(0, HALF - 1)], m.r_x.at[h])
+
+        @pl.when(jnp.logical_not(inside))
+        def _():
+            wait(m.x.at[pl.ds(0, HALF)], m.r_x.at[h])
+
+        m.slots[h] = (
+            dot(
+                m.place[h],
+                m.x[HALF * h : HALF * (h + 1)].reshape(HALF * ROWS, 2 * COLS),
+            )
+            .astype(BF16)
+            .reshape(NE, UNIT, 2 * COLS)
         )
-        named = jnp.zeros((NE, 128), F32)
-        share = jnp.zeros((NE, 128), F32)
-        for n in range(6):
-            hit = chosen[n : n + 1] == expert
-            named = jnp.where(hit, 1.0, named)
-            share = jnp.where(hit, shares[n : n + 1], share)
-        a = lax.broadcasted_iota(jnp.int32, (128, 128), 0)
-        b = lax.broadcasted_iota(jnp.int32, (128, 128), 1)
-        ahead = jnp.where((a // ROWS == b // ROWS) & (a < b), 1.0, 0.0).astype(BF16)
-        rank = dot(named.astype(BF16), ahead)
-        code = jnp.where(named > 0.5, rank + (2 * (lane // ROWS)).astype(F32), -1.0)
-        slot = lax.broadcasted_iota(jnp.int32, (ROWS, 128), 0).astype(F32)
-        for n in range(NE):
-            hit = code[n : n + 1] == slot
-            m.place[pl.ds(ROWS * n, ROWS), :] = jnp.where(hit, 1.0, 0.0).astype(BF16)
-            m.weigh[pl.ds(ROWS * n, ROWS), :] = jnp.where(hit, share[n : n + 1], 0.0).astype(BF16)
-
-    def dispatch():
-        wait(m.x.at[pl.ds(1, NY - 1)], m.r_x)
-        m.slots[...] = (
-            dot(m.place[...], m.x[...].reshape(NY * ROWS, 2 * COLS))
-            .astype(BF16)
-            .reshape(NE, ROWS, 2 * COLS)
-        )
-        for spot, d in enumerate(ORDER):
+        wave = c * h + (1 - c) * near_half
+        for d in FAR + (0,):
+            spot = c * (NE // 2 + (NZ - d) % NZ) + (1 - c) * (2 * ((NZ - d) % HALF) + h)
             for e in range(NC):
-                k = NC * ((NZ - d) % NZ) + e
+                k = lax.rem(mine_b + d, NZ) * 2 + lax.rem(c + e, NC)
                 if d or e:
                     send(
-                        m.slots.at[k],
-                        m.got.at[NC * spot + e, :, left],
+                        m.slots.at[h, k],
+                        m.got.at[wave, spot, :, left],
                         m.s_z,
-                        m.r_z.at[chunk_of(spot)],
-                        at(b=(NZ - d) % NZ, dc=e),
+                        m.r_z.at[2 * wave + c],
+                        at(b=d, dc=e),
                     )
                 else:
-                    m.got[NC * spot, :, left] = m.slots[k]
-
-    def trade(n):
-        if n == 0:
-            wait(m.wgu, m.loc.at[15])
-        lo, hi = CHUNKS[n]
-        some = pl.ds(NC * lo, NC * (hi - lo))
-        fresh = pl.ds(NC * lo, NC * (hi - lo) - (lo <= ORDER.index(0) < hi))
-        wait(m.got.at[fresh, :, left], m.r_z.at[n])
-        for k, d in ((0, 1), (1, 3)):
+                    m.got[wave, spot, :, left] = m.slots[h, k]
+
+    def up_ready():
+        wait(m.wgu, m.loc.at[15])
+
+    def down_ready():
+        wait(m.wdn.at[0], m.loc.at[10])
+        wait(m.wdn.at[pl.ds(1, NT - 1)], m.r_wdn)
+
+    def trade(w, k):
+        n, begin, count = 2 * w + k, NE // 2 * k, NE // 2
+        own = (near_half == w) & (c == 0) if k == 0 else c == 1
+
+        @pl.when(own)
+        def _():
+            wait(m.got.at[w, pl.ds(begin, count - (2 - k)), :, left], m.r_z.at[n])
+
+        @pl.when(jnp.logical_not(own))
+        def _():
+            wait(m.got.at[w, pl.ds(begin, count), :, left], m.r_z.at[n])
+
+        some = pl.ds(begin, count)
+        for j, d in ((0, 1), (1, 3)):
             send(
-                m.got.at[some, :, pl.ds(COLS * k, COLS)],
-                m.got.at[some, :, pl.ds(COLS * (3 - k), COLS)],
+                m.got.at[w, some, :, pl.ds(COLS * j, COLS)],
+                m.got.at[w, some, :, pl.ds(COLS * (3 - j), COLS)],
                 m.s_up,
                 m.r_up.at[n],
                 at(dt=d),
             )
-        size = NC * ROWS * (hi - lo)
-        m.half[pl.ds(NC * ROWS * lo, size)] = dot(
-            m.got[NC * lo : NC * hi, :, 0 : 2 * COLS].reshape(size, 2 * COLS),
+        m.half[w, pl.ds(UNIT * begin, UNIT * count)] = dot(
+            m.got[w, begin : begin + count, :, 0 : 2 * COLS].reshape(count * UNIT, 2 * COLS),
             m.wgu[0 : 2 * COLS],
         )
 
-    def hide(n):
-        lo, hi = CHUNKS[n]
-        size = NC * ROWS * (hi - lo)
-        span = pl.ds(NC * ROWS * lo, size)
-        wait(m.got.at[pl.ds(NC * lo, NC * (hi - lo)), :, right], m.r_up.at[n])
-        total = m.half[span] + dot(
-            m.got[NC * lo : NC * hi, :, 2 * COLS :].reshape(size, 2 * COLS),
+    def hide(w, k):
+        n, begin, count = 2 * w + k, NE // 2 * k, NE // 2
+        span = pl.ds(UNIT * begin, UNIT * count)
+        wait(m.got.at[w, pl.ds(begin, count), :, right], m.r_up.at[n])
+        total = m.half[w, span] + dot(
+            m.got[w, begin : begin + count, :, 2 * COLS :].reshape(count * UNIT, 2 * COLS),
             m.wgu[2 * COLS :],
         )
         pre = total[:, :HID]
         hidden = (pre / (1.0 + jnp.exp(-pre)) * total[:, HID:]).astype(BF16)
-        m.hid[span] = hidden
-        m.hids[span, 0:HID] = hidden
+        m.hid[w, span] = hidden
+        m.hids[w, span, 0:HID] = hidden
         for d in (2, 1, 3):
             send(
-                m.hid.at[span],
-                m.hids.at[span, pl.ds(HID * (NT - d), HID)],
+                m.hid.at[w, span],
+                m.hids.at[w, span, pl.ds(HID * (NT - d), HID)],
                 m.s_ag,
                 m.r_ag.at[n],
                 at(dt=d),
             )
 
-    def answer(n):
-        if n == 0:
-            wait(m.wdn.at[0], m.loc.at[10])
-            wait(m.wdn.at[pl.ds(1, NT - 1)], m.r_wdn)
-        lo, hi = CHUNKS[n]
-        size = NC * ROWS * (hi - lo)
-        span = pl.ds(NC * ROWS * lo, size)
-        wait(m.hids.at[span, pl.ds(HID, (NT - 1) * HID)], m.r_ag.at[n])
-        m.rows[NC * lo : NC * hi] = (
-            dot(m.hids[span], m.wdn[...].reshape(NT * HID, COLS))
+    def answer(w, k):
+        n, begin, count = 2 * w + k, NE // 2 * k, NE // 2
+        span = pl.ds(UNIT * begin, UNIT * count)
+        wait(m.hids.at[w, span, pl.ds(HID, (NT - 1) * HID)], m.r_ag.at[n])
+        m.rows[w, begin : begin + count] = (
+            dot(m.hids[w, span], m.wdn[...].reshape(NT * HID, COLS))
             .astype(BF16)
-            .reshape(NC * (hi - lo), ROWS, COLS)
+            .reshape(count, UNIT, COLS)
         )
-        for spot in range(lo, hi):
-            d = ORDER[spot]
-            for e in range(NC):
-                if d or e:
-                    send(
-                        m.rows.at[NC * spot + e],
-                        m.back.at[NC * ((NZ - d) % NZ) + e],
-                        m.s_rz,
-                        m.r_rz,
-                        at(a=d, dc=1) if e else at(b=d),
-                    )
-                else:
-                    m.back[0] = m.rows[NC * spot]
+
+        def reply(spot, to, h, k):
+            send(m.rows.at[w, spot], m.back.at[h, k], m.s_rz, m.r_rz.at[h], (to, t))
+
+        for d in (2, 1, 3, 0) if k == 0 else ():
+            to = (HALF * w + lax.rem(z + d, HALF)) * 16 + y * 2
+            for h in range(2):
+                spot, e = 2 * d + h, z * 2 + c
+                if d:
+                    reply(spot, to, h, e)
+                    continue
+                own = (c == 0) & (near_half == w)
+
+                @pl.when(jnp.logical_not(own))
+                def _(spot=spot, to=to, h=h, e=e):
+                    reply(spot, to, h, e)
+
+                @pl.when(own)
+                def _(spot=spot, h=h, e=e):
+                    m.back[h, e] = m.rows[w, spot]
+
+        for d in FAR + (0,) if k == 1 else ():
+            to = z * 16 + lax.rem(y + d, NY) * 2 + 1
+            spot, e = NE // 2 + d, y * 2 + c
+            if d:
+                reply(spot, to, w, e)
+                continue
+
+            @pl.when(c == 0)
+            def _(spot=spot, to=to, e=e):
+                reply(spot, to, w, e)
+
+            @pl.when(c == 1)
+            def _(spot=spot, e=e):
+                m.back[w, e] = m.rows[w, spot]
+
+    def combine(h):
+        wait(m.back.at[h, pl.ds(0, NE - 1)], m.r_rz.at[h])
+        both = dot_tn(m.weigh[h], m.back[h].reshape(NE * UNIT, COLS))
+        m.acc[HALF * h : HALF * (h + 1)] = both.astype(BF16).reshape(HALF, ROWS, COLS)
+        for d in (2, 1, 3, 0):
+            a = HALF * h + lax.rem(mine_a + d, HALF)
+            to = ((z * (1 - c) + a * c) * 16 + (y * c + a * (1 - c)) * 2 + c, t)
+
+            def reply(a=a, to=to):
+                send(m.acc.at[a], m.fin.at[mine_a], m.s_y, m.r_y, to)
+
+            if d:
+                reply()
+                continue
+            own = mine_a // HALF == h
+
+            @pl.when(jnp.logical_not(own))
+            def _(reply=reply):
+                reply()
+
+            @pl.when(own)
+            def _():
+                m.fin[mine_a] = m.acc[mine_a]
 
     def dense_in():
         wait(m.dx, m.r_dx)
@@ -477,22 +548,19 @@
             .reshape(NC * NY, ROWS, COLS)
         )
         for d in FAR + (0,):
+            a = lax.rem(mine_a + d, NY)
             for e in range(NC):
                 if d or e:
                     send(
-                        m.dacc.at[NY * e + d],
-                        m.dfin.at[NY * e + (NY - d) % NY],
+                        m.dacc.at[NY * e + a],
+                        m.dfin.at[NY * e + mine_a],
                         m.s_dy,
                         m.r_dy,
                         at(a=d, dc=e),
                     )
+        m.dfin[mine_a] = m.dacc[mine_a]
 
     def finish():
-        wait(m.back.at[pl.ds(1, NE - 1)], m.r_rz)
-        both = dot_tn(m.weigh[...], m.back[...].reshape(NE * ROWS, COLS))
-        m.acc[...] = both.astype(BF16).reshape(NY, ROWS, COLS)
-        for d in FAR:
-            send(m.acc.at[d], m.fin.at[NY - d], m.s_y, m.r_y, at(a=d))
         wait(m.bgate, m.loc.at[14])
         gate = m.bgate[...].astype(F32)
         branch = jnp.zeros((ROWS, 128), F32)
@@ -501,12 +569,12 @@
         branch = jnp.sum(branch, axis=1, keepdims=True)
         branch = 1.0 / (1.0 + jnp.exp(-branch))
         wait(m.dfin.at[pl.ds(1, NC * NY - 1)], m.r_dy)
-        total = m.dacc[0].astype(F32)
+        total = m.dfin[0].astype(F32)
         for d in range(1, NC * NY):
             total = total + m.dfin[d].astype(F32)
-        total = m.after[:, block(0)] + branch * total + m.acc[0].astype(F32)
+        total = m.after[:, block(0)] + branch * total
         wait(m.fin.at[pl.ds(1, NY - 1)], m.r_y)
-        for d in range(1, NY):
+        for d in range(NY):
             total = total + m.fin[d].astype(F32)
         out[...] = total.astype(BF16)
 
@@ -530,23 +598,32 @@
     gather_other()
     split_down()
     assign()
-    dispatch()
+    pl.when((c == 1) | (near_half == 0))(lambda: emit(0))
+    pl.when((c == 0) & (near_half == 0))(lambda: emit(1))
+    pl.when((c == 0) & (near_half == 1))(lambda: emit(0))
+    pl.when((c == 1) | (near_half == 1))(lambda: emit(1))
     dense_in()
-    trade(0)
-    trade(1)
-    trade(2)
-    trade(3)
+    up_ready()
+    trade(0, 1)
+    trade(0, 0)
+    trade(1, 1)
+    trade(1, 0)
     spread(2)
-    hide(0)
-    hide(1)
-    hide(2)
-    hide(3)
+    hide(0, 1)
+    hide(0, 0)
+    hide(1, 1)
+    hide(1, 0)
     dense_hide()
-    answer(0)
-    answer(1)
-    answer(2)
-    answer(3)
+    down_ready()
+    answer(0, 1)
+    answer(0, 0)
+    answer(1, 1)
+    answer(1, 0)
     dense_out()
+    pl.when((c == 1) | (near_half == 0))(lambda: combine(0))
+    pl.when((c == 0) & (near_half == 0))(lambda: combine(1))
+    pl.when((c == 0) & (near_half == 1))(lambda: combine(0))
+    pl.when((c == 1) | (near_half == 1))(lambda: combine(1))
     finish()
 
     wait(m.hp.at[pl.ds(1, NT - 1)], m.s_hp)
@@ -557,12 +634,12 @@
     wait(m.dx, m.s_dx)
     for k in range(3):
         wait(dense[k].at[pl.ds(1, NZ - 1)], m.s_dw.at[k])
-    wait(m.got.at[pl.ds(1, NE - 1), :, left], m.s_z)
-    wait(m.got.at[:, :, right], m.s_up)
-    wait(m.hids.at[:, pl.ds(HID, (NT - 1) * HID)], m.s_ag)
+    wait(m.slots.at[:, pl.ds(0, NE - 1)], m.s_z)
+    wait(m.got.at[:, :, :, right], m.s_up)
+    wait(m.hids.at[:, :, pl.ds(HID, (NT - 1) * HID)], m.s_ag)
     wait(m.dparts.at[pl.ds(1, NT - 1)], m.s_drs)
     wait(m.dhids.at[pl.ds(0, 2 * gathered - quarter)], m.s_dag)
-    wait(m.back.at[pl.ds(1, NE - 1)], m.s_rz)
+    wait(m.back.at[:, pl.ds(0, NE - 1)], m.s_rz)
     wait(m.dfin.at[pl.ds(1, NC * NY - 1)], m.s_dy)
     wait(m.fin.at[pl.ds(1, NY - 1)], m.s_y)
 

time: 56.1 us -> 53.9 us (0.961)
  Pallas kernels: 55.4 us -> 52.8 us
    pallas_call x1, Pallas kernels: 55.4 us -> 52.8 us  [on_device(): pl.pallas_call(kernel, name='layer', out_shape=pltpu.VMEM((ROWS, COLS), B...]
where the time goes in v6:
time: 53.9 us; the launch traced here: 53.5 us
  Pallas kernels  52.8 us (98%)
  local copies, waits for them, and re-layouts  0.61 us (1%)
    pallas_call x1, Pallas kernels, on_device(): pl.pallas_call(kernel, name='layer', out_shape=pltpu.VMEM((ROWS, COLS), B...  52.8 us

profile of v6, /device:TPU:1, one launch (start us, length us, event | category | flops | bytes accessed | tf_op | source)
XLA Modules:
  0.0 53.5 jit_solution(14026224583292749764)
XLA Ops:
  0.0 52.8 %layer.1 = bf16[16,512]{1,0:T(8,128)(2,1)S(1)} custom-call(bf16[16,2048]{1,0:T(8,128)(2,1)} %tokens.1, s32[1,16]{1,0:T(1,128)} %bitcast.23, f32[16,128,128]{2,1,0:T(8,128)} %bitcast.12, f32[16,128]{1,0:T(8,128)} %bitcast.18, bf16[2048,128]{1,0:T(8,128)(2,1)} %w_query.1, bf16[2048,128]{1,0:T(8,128)(2,1)} %w_key.1, bf16[2048,128]{1,0:T(8,128)(2,1)} %w_value.1, ...), custom_call_target="tpu_custom_call" | custom-call | tf_op jit(solution)/shard_map/layer/pallas_call | solution.py:691
  52.8 0.6 %copy.21 = bf16[16,512]{1,0:T(8,128)(2,1)} copy(bf16[16,512]{1,0:T(8,128)(2,1)S(1)} %layer.1) | data formatting | bytes 32768

commit v7 on v6

--- a/solution.py
+++ b/solution.py
@@ -374,7 +374,7 @@
             .reshape(NE, UNIT, 2 * COLS)
         )
         wave = c * h + (1 - c) * near_half
-        for d in FAR + (0,):
+        for d in (1, 7, 4, 3, 5, 2, 6) + (0,):
             spot = c * (NE // 2 + (NZ - d) % NZ) + (1 - c) * (2 * ((NZ - d) % HALF) + h)
             for e in range(NC):
                 k = lax.rem(mine_b + d, NZ) * 2 + lax.rem(c + e, NC)
@@ -547,7 +547,7 @@
             .astype(BF16)
             .reshape(NC * NY, ROWS, COLS)
         )
-        for d in FAR + (0,):
+        for d in (2, 6, 4, 3, 5, 1, 7) + (0,):
             a = lax.rem(mine_a + d, NY)
             for e in range(NC):
                 if d or e:

time: 53.9 us -> 53.9 us (level)
  no operation moved by 1% of the time
where the time goes in v7:
time: 53.9 us; the launch traced here: 53.6 us
  Pallas kernels  53 us (98%)
  local copies, waits for them, and re-layouts  0.61 us (1%)
    pallas_call x1, Pallas kernels, on_device(): pl.pallas_call(kernel, name='layer', out_shape=pltpu.VMEM((ROWS, COLS), B...  53 us

profile of v7, /device:TPU:1, one launch (start us, length us, event | category | flops | bytes accessed | tf_op | source)
XLA Modules:
  0.0 53.6 jit_solution(2410826689243103208)
XLA Ops:
  0.0 53.0 %layer.1 = bf16[16,512]{1,0:T(8,128)(2,1)S(1)} custom-call(bf16[16,2048]{1,0:T(8,128)(2,1)} %tokens.1, s32[1,16]{1,0:T(1,128)} %bitcast.23, f32[16,128,128]{2,1,0:T(8,128)} %bitcast.12, f32[16,128]{1,0:T(8,128)} %bitcast.18, bf16[2048,128]{1,0:T(8,128)(2,1)} %w_query.1, bf16[2048,128]{1,0:T(8,128)(2,1)} %w_key.1, bf16[2048,128]{1,0:T(8,128)(2,1)} %w_value.1, ...), custom_call_target="tpu_custom_call" | custom-call | tf_op jit(solution)/shard_map/layer/pallas_call | solution.py:691
  53.0 0.6 %copy.21 = bf16[16,512]{1,0:T(8,128)(2,1)} copy(bf16[16,512]{1,0:T(8,128)(2,1)S(1)} %layer.1) | data formatting | bytes 32768
